TPU v7x, 32 devices: a whole 2x2x4 slice. The times are simulated.
32 devices in a mesh: ep: 4 (over z), tp: 8 (over y, x, core).
Axes of the slice: x: 2, y: 2, z: 4, core: 2. Of those that a mesh axis runs over, the one named last changes fastest.
Arguments:
- tokens: bfloat16 [640, 2048], P('ep', 'tp'), may hold values from -6 to 6
- cotangent: bfloat16 [640, 2048], P('ep', 'tp'), may hold values from -6 to 6
- routes: int32 [640, 2], P('ep'), may hold values from 0 to 23, all different within a row; in each aligned block of 160 rows (0 to 159, 160 to 319, ...) at most 14 rows name the same one
- gate_weights: float32 [640, 2], P('ep'), may hold values from 0.2 to 2.5
- expert_gate: bfloat16 [24, 2048, 512], P('ep', 'tp'), may hold values from -0.125 to 0.125
- expert_up: bfloat16 [24, 2048, 512], P('ep', 'tp'), may hold values from -0.125 to 0.125
- expert_down: bfloat16 [24, 512, 2048], P('ep', None, 'tp'), may hold values from -0.25 to 0.25
- shared_gate: bfloat16 [2048, 576], P('tp'), may hold values from -0.125 to 0.125
- shared_up: bfloat16 [2048, 576], P('tp'), may hold values from -0.125 to 0.125
- shared_down: bfloat16 [576, 2048], P(None, 'tp'), may hold values from -0.25 to 0.25
Outputs:
- token_grad: bfloat16 [640, 2048], P('ep', 'tp')
- weight_grad: float32 [640, 2], P('ep')
- expert_gate_grad: float32 [24, 2048, 512], P('ep', 'tp')
- expert_up_grad: float32 [24, 2048, 512], P('ep', 'tp')
- expert_down_grad: float32 [24, 512, 2048], P('ep', None, 'tp')
- shared_gate_grad: float32 [2048, 576], P('tp', 'ep')
- shared_up_grad: float32 [2048, 576], P('tp', 'ep')
- shared_down_grad: float32 [576, 2048], P('ep', 'tp')
- gate_rows_sq: float32 [24, 2048], P('ep', 'tp')
- up_rows_sq: float32 [24, 2048], P('ep', 'tp')
- down_rows_sq: float32 [24, 512], P('ep')
- shared_gate_rows_sq: float32 [2048], P('tp')
- shared_up_rows_sq: float32 [2048], P('tp')
- shared_down_rows_sq: float32 [576], P('ep')
Inputs may be any that keep to these rules, and one draw needn't show every extreme that they name: `routes`: each row names 2 different experts. Among the rows of one index of ep (aligned blocks of 160 rows) no expert is named more than 14 times, a bound that some block reaches.
All inputs are finite; a program needn't handle non-finite values.
Results may differ from a plain program's by a relative error of at most 0.0059.
Values may be sent and summed in bfloat16 or wider, within the bound.
A program may use at most 64 MiB of HBM per device.

v0:
```python
import jax
import jax.numpy as jnp
from jax import lax
from jax.sharding import PartitionSpec as P


def silu_parts(pre):
    logistic = jax.nn.sigmoid(pre)
    return (pre * logistic, logistic * (1.0 + pre * (1.0 - logistic)))


def activate(gate_sum, up_sum, back_sum, recv_w, s_gate, s_up, s_back):
    silu_out, silu_slope = silu_parts(gate_sum)
    hidden = (silu_out * up_sum).astype(jnp.bfloat16)
    dhidden = recv_w[:, :, None] * back_sum
    grad_gate = (dhidden * up_sum * silu_slope).astype(jnp.bfloat16)
    grad_up = (dhidden * silu_out).astype(jnp.bfloat16)
    dots = jnp.sum(hidden.astype(jnp.float32) * back_sum, axis=2)
    s_out, s_slope = silu_parts(s_gate)
    s_hidden = (s_out * s_up).astype(jnp.bfloat16)
    s_dgate = (s_back * s_up * s_slope).astype(jnp.bfloat16)
    s_dup = (s_back * s_out).astype(jnp.bfloat16)
    return (hidden, grad_gate, grad_up, dots, s_hidden, s_dgate, s_dup)


def per_device(
    tokens,
    cotangent,
    routes,
    gate_weights,
    expert_gate,
    expert_up,
    expert_down,
    shared_gate,
    shared_up,
    shared_down,
):
    tok_rows, narrow = tokens.shape
    picks_per = routes.shape[1]
    local_experts = expert_gate.shape[0]
    experts_all = local_experts * lax.axis_size("ep")
    capacity = max(2, (tok_rows * picks_per + experts_all - 1) // experts_all)
    owners = routes.reshape(-1)
    assigned = owners.shape[0]
    picked = (owners[:, None] == jnp.arange(experts_all, dtype=jnp.int32)[None, :]).astype(
        jnp.int32
    )
    slot_rank = jnp.sum((jnp.cumsum(picked, axis=0) - picked) * picked, axis=1)
    source_tok = jnp.arange(assigned, dtype=jnp.int32) // picks_per
    slot_tok = (
        jnp.full((capacity, experts_all), tok_rows, jnp.int32).at[slot_rank, owners].set(source_tok)
    )
    slot_weight = (
        jnp.zeros((capacity, experts_all), jnp.float32)
        .at[slot_rank, owners]
        .set(gate_weights.reshape(-1))
    )
    zero_row = jnp.zeros((1, narrow), tokens.dtype)
    sent_x = jnp.concatenate([tokens, zero_row], axis=0)[slot_tok]
    sent_dy = jnp.concatenate([cotangent, zero_row], axis=0)[slot_tok]
    recv_x, recv_dy = (
        lax.all_to_all(sent_x, "ep", split_axis=1, concat_axis=0, tiled=True),
        lax.all_to_all(sent_dy, "ep", split_axis=1, concat_axis=0, tiled=True),
    )
    recv_w = lax.all_to_all(slot_weight, "ep", split_axis=1, concat_axis=0, tiled=True)
    gate_part = jnp.einsum("rel,elf->ref", recv_x, expert_gate, preferred_element_type=jnp.float32)
    up_part = jnp.einsum("rel,elf->ref", recv_x, expert_up, preferred_element_type=jnp.float32)
    back_part = jnp.einsum("rel,efl->ref", recv_dy, expert_down, preferred_element_type=jnp.float32)
    s_gate_part = jnp.dot(tokens, shared_gate, preferred_element_type=jnp.float32)
    s_up_part = jnp.dot(tokens, shared_up, preferred_element_type=jnp.float32)
    s_back_part = jnp.einsum(
        "tl,sl->ts", cotangent, shared_down, preferred_element_type=jnp.float32
    )
    gate_sum, up_sum, back_sum, s_gate, s_up, s_back = lax.psum(
        (gate_part, up_part, back_part, s_gate_part, s_up_part, s_back_part), "tp"
    )
    hidden, grad_gate, grad_up, gate_grad, s_hidden, s_dgate, s_dup = activate(
        gate_sum, up_sum, back_sum, recv_w, s_gate, s_up, s_back
    )
    weighted = (recv_w[:, :, None] * recv_dy.astype(jnp.float32)).astype(jnp.bfloat16)
    down_grad = jnp.einsum("ref,rel->efl", hidden, weighted, preferred_element_type=jnp.float32)
    gate_wgrad = jnp.einsum("rel,ref->elf", recv_x, grad_gate, preferred_element_type=jnp.float32)
    up_wgrad = jnp.einsum("rel,ref->elf", recv_x, grad_up, preferred_element_type=jnp.float32)
    row_grad = (
        jnp.einsum("ref,elf->rel", grad_gate, expert_gate, preferred_element_type=jnp.float32)
        + jnp.einsum("ref,elf->rel", grad_up, expert_up, preferred_element_type=jnp.float32)
    ).astype(jnp.bfloat16)
    back_rows = lax.all_to_all(row_grad, "ep", split_axis=0, concat_axis=1, tiled=True)
    back_gate = lax.all_to_all(gate_grad, "ep", split_axis=0, concat_axis=1, tiled=True)
    flat_index = slot_rank * experts_all + owners
    routed = back_rows.reshape(capacity * experts_all, narrow)[flat_index].astype(jnp.float32)
    routed = routed.reshape(tok_rows, picks_per, narrow).sum(axis=1)
    weight_grad = back_gate.reshape(-1)[flat_index].reshape(tok_rows, picks_per)
    term_gate = jnp.einsum("tl,ts->ls", tokens, s_dgate, preferred_element_type=jnp.float32)
    term_up = jnp.einsum("tl,ts->ls", tokens, s_dup, preferred_element_type=jnp.float32)
    term_down = jnp.einsum("ts,tl->sl", s_hidden, cotangent, preferred_element_type=jnp.float32)
    shared_gate_grad, shared_up_grad, shared_down_grad = (
        lax.psum_scatter(term_gate, "ep", scatter_dimension=1, tiled=True),
        lax.psum_scatter(term_up, "ep", scatter_dimension=1, tiled=True),
        lax.psum_scatter(term_down, "ep", scatter_dimension=0, tiled=True),
    )
    shared_rows = jnp.einsum(
        "ts,ls->tl", s_dgate, shared_gate, preferred_element_type=jnp.float32
    ) + jnp.einsum("ts,ls->tl", s_dup, shared_up, preferred_element_type=jnp.float32)
    token_grad = (routed + shared_rows).astype(jnp.bfloat16)
    gate_rows_sq = jnp.sum(gate_wgrad * gate_wgrad, axis=2)
    up_rows_sq = jnp.sum(up_wgrad * up_wgrad, axis=2)
    down_rows_sq, shared_down_rows_sq = lax.psum(
        (
            jnp.sum(down_grad * down_grad, axis=2),
            jnp.sum(shared_down_grad * shared_down_grad, axis=1),
        ),
        "tp",
    )
    shared_gate_rows_sq, shared_up_rows_sq = lax.psum(
        (
            jnp.sum(shared_gate_grad * shared_gate_grad, axis=1),
            jnp.sum(shared_up_grad * shared_up_grad, axis=1),
        ),
        "ep",
    )
    return (
        token_grad,
        weight_grad,
        gate_wgrad,
        up_wgrad,
        down_grad,
        shared_gate_grad,
        shared_up_grad,
        shared_down_grad,
        gate_rows_sq,
        up_rows_sq,
        down_rows_sq,
        shared_gate_rows_sq,
        shared_up_rows_sq,
        shared_down_rows_sq,
    )


def solution(mesh):
    return jax.shard_map(
        per_device,
        mesh=mesh,
        in_specs=(
            P("ep", "tp"),
            P("ep", "tp"),
            P("ep", None),
            P("ep", None),
            P("ep", "tp", None),
            P("ep", "tp", None),
            P("ep", None, "tp"),
            P("tp", None),
            P("tp", None),
            P(None, "tp"),
        ),
        out_specs=(
            P("ep", "tp"),
            P("ep", None),
            P("ep", "tp", None),
            P("ep", "tp", None),
            P("ep", None, "tp"),
            P("tp", "ep"),
            P("tp", "ep"),
            P("ep", "tp"),
            P("ep", "tp"),
            P("ep", "tp"),
            P("ep", None),
            P("tp"),
            P("tp"),
            P("ep"),
        ),
        check_vma=False,
    )
```

profile of v0, /device:TPU:0, one launch (start us, length us, event | category | flops | bytes accessed | tf_op | source)
XLA Modules:
  0.0 251.2 jit_solution(17227434565805106463)
XLA Ops:
  9.7 17.0 %scatter_fusion.1 = s32[14,24]{1,0:T(8,128)S(1)} fusion(s32[14,24]{1,0:T(8,128)S(1)} %broadcast_in_dim.7, s32[320]{0:T(512)S(1)} %get-tuple-element.71, s32[320]{0:T(512)S(1)} %add_select_fusion), kind=kCustom, calls=%fused_computation.5 | custom fusion | bytes 6400 | tf_op jit(solution)/shard_map/scatter | solution.py:51
  26.9 2.0 gather_fusion.1
  29.7 6.3 %all-to-all-start.2 = ((bf16[14,24,256]{2,0,1:T(8,128)(2,1)}), bf16[14,24,256]{2,0,1:T(8,128)(2,1)S(1)}, u32[]{:S(2)}, u32[]{:S(2)}) async-start(bf16[14,24,256]{2,0,1:T(8,128)(2,1)} %copy.65), calls=%async_computation.2 | async-start | bytes 393216 | tf_op jit(solution)/shard_map/all_to_all | solution.py:62
  38.1 2.0 gather_fusion
  41.9 1.7 all-to-all-done.2
  43.5 4.0 %all-to-all-start.1 = ((bf16[14,24,256]{2,0,1:T(8,128)(2,1)}), bf16[14,24,256]{2,0,1:T(8,128)(2,1)}, u32[]{:S(2)}, u32[]{:S(2)}) async-start(bf16[14,24,256]{2,0,1:T(8,128)(2,1)} %copy.63), calls=%async_computation.1 | async-start | bytes 393216 | tf_op jit(solution)/shard_map/all_to_all | solution.py:63
  47.6 1.7 copy.66
  50.3 1.2 convolution_bitcast_fusion
  51.6 1.2 convolution_bitcast_fusion.1
  53.8 1.6 copy.64
  55.5 1.7 all_to_all.67
  57.1 3.0 %convolution_bitcast_fusion.2 = f32[56,6,512]{2,0,1:T(8,128)} fusion(bf16[56,6,256]{2,0,1:T(8,128)(2,1)} %all_to_all.67, bf16[6,512,256]{2,1,0:T(8,128)(2,1)} %param.16), kind=kOutput, calls=%fused_computation.11 | convolution fusion | flops 88080384 | bytes 2433024 | tf_op jit(solution)/shard_map/rel,efl->ref/dot_general | solution.py:68
  60.2 72.4 %all-reduce.8.cloned.1.call-done = (f32[56,6,512]{2,0,1:T(8,128)}, f32[56,6,512]{2,0,1:T(8,128)}, f32[56,6,512]{2,0,1:T(8,128)}, f32[160,576]{1,0:T(8,128)}, f32[160,576]{1,0:T(8,128)}, /*index=5*/f32[160,576]{1,0:T(8,128)}) async-done(((f32[56,6,512]{2,0,1:T(8,128)}, f32[56,6,512]{2,0,1:T(8,128)}, f32[56,6,512]{2,0,1:T(8,128)}, f32[160,576]{1,0:T(8,128)}, f32[160,576]{1,0:T(8,128)}, ...) | async-done | bytes 3170320 | tf_op jit(solution)/shard_map/psum | solution.py:74
  132.6 2.2 fusion.6
  135.2 17.0 %scatter_fusion = f32[14,24]{1,0:T(8,128)S(1)} fusion(f32[14,24]{1,0:T(8,128)S(1)} %broadcast_in_dim.6, s32[320]{0:T(512)S(1)} %get-tuple-element.71, f32[320]{0:T(512)S(1)} %reshape.179), kind=kCustom, calls=%fused_computation.4 | custom fusion | bytes 6400 | tf_op jit(solution)/shard_map/scatter | solution.py:56
  152.9 4.6 %all-to-all-start = ((f32[14,4,6]{0,2,1:T(8,128)}), f32[14,4,6]{0,2,1:T(8,128)S(1)}, u32[]{:S(2)}, u32[]{:S(2)}) async-start(f32[14,4,6]{0,2,1:T(8,128)} %all_to_all.61), calls=%async_computation | async-start | bytes 32768 | tf_op jit(solution)/shard_map/all_to_all | solution.py:65
  157.5 5.6 %all-to-all-done = f32[14,4,6]{0,2,1:T(8,128)S(1)} async-done(((f32[14,4,6]{0,2,1:T(8,128)}), f32[14,4,6]{0,2,1:T(8,128)S(1)}, u32[]{:S(2)}, u32[]{:S(2)}) %all-to-all-start) | async-done | bytes 1376 | tf_op jit(solution)/shard_map/all_to_all | solution.py:65
  163.2 2.1 multiply_convert_fusion.4
  167.1 2.9 %multiply_reduce_fusion.3 = (f32[56,6]{0,1:T(8,128)S(1)}, bf16[56,6,512]{2,0,1:T(8,128)(2,1)}, bf16[56,6,512]{2,0,1:T(8,128)(2,1)}, bf16[56,6,512]{2,0,1:T(8,128)(2,1)}) fusion(f32[56,6,512]{2,0,1:T(8,128)} %get-tuple-element.76, f32[56,6,512]{2,0,1:T(8,128)} %get-tuple-element.75, f32[56,6,512]{2,0,1:T(8,128)} %get-tuple-element.74, f32[56,6]{0,1:T(8,128)S(1)} %mul.95), kind=kLoop, calls=%fused_computation.20 | loop fusion | flops 3268272 | bytes 3099264 | tf_op jit(solution)/shard_map/reduce_sum | solution.py:18
  170.7 3.3 %all-to-all-start.4 = ((f32[4,14,6]{1,2,0:T(8,128)}), f32[4,14,6]{1,2,0:T(8,128)S(1)}, u32[]{:S(2)}, u32[]{:S(2)}) async-start(f32[4,14,6]{1,2,0:T(8,128)} %copy.70), calls=%async_computation.4 | async-start | bytes 32768 | tf_op jit(solution)/shard_map/all_to_all | solution.py:89
  174.0 2.0 convolution_bitcast_fusion.4
  176.0 2.4 fusion.19
  178.4 2.9 %multiply_reduce_fusion.2 = (f32[6,256]{1,0:T(8,128)}, f32[6,256,512]{2,1,0:T(8,128)}) fusion(bf16[56,6,256]{2,0,1:T(8,128)(2,1)S(1)} %all_to_all.71, bf16[56,6,512]{2,0,1:T(8,128)(2,1)S(1)} %copy-done.2), kind=kOutput, calls=%fused_computation.8 | convolution fusion | flops 89651712 | bytes 3667968 | tf_op jit(solution)/shard_map/rel,ref->elf/dot_general | solution.py:82
  181.3 2.5 %multiply_reduce_fusion = (f32[6,512]{1,0:T(8,128)S(1)}, f32[6,512,256]{1,2,0:T(8,128)}) fusion(bf16[56,6,512]{2,0,1:T(8,128)(2,1)S(1)} %copy-done.8, bf16[56,6,256]{2,0,1:T(8,128)(2,1)S(1)} %copy-done.7, f32[56,6]{0,1:T(8,128)S(1)} %mul.95), kind=kOutput, calls=%fused_computation.6 | convolution fusion | flops 89908224 | bytes 3675456 | tf_op jit(solution)/shard_map/ref,rel->efl/dot_general | solution.py:81
  183.9 1.7 fusion.1
  186.3 5.0 %all-to-all-start.3 = ((bf16[56,6,256]{2,1,0:T(8,128)(2,1)}), bf16[56,6,256]{2,1,0:T(8,128)(2,1)S(1)}, u32[]{:S(2)}, u32[]{:S(2)}) async-start(bf16[56,6,256]{2,1,0:T(8,128)(2,1)} %copy.67), calls=%async_computation.3 | async-start | bytes 458752 | tf_op jit(solution)/shard_map/all_to_all | solution.py:88
  191.3 3.9 %multiply_reduce_fusion.1 = (f32[6,256]{1,0:T(8,128)}, f32[6,256,512]{2,1,0:T(8,128)}) fusion(bf16[56,6,256]{2,0,1:T(8,128)(2,1)S(1)} %all_to_all.71, bf16[56,6,512]{2,0,1:T(8,128)(2,1)} %get-tuple-element.85), kind=kOutput, calls=%fused_computation.7 | convolution fusion | flops 89651712 | bytes 3667968 | tf_op jit(solution)/shard_map/rel,ref->elf/dot_general | solution.py:83
  195.2 3.6 %copy.73 = f32[6,512,256]{2,1,0:T(8,128)} copy(f32[6,512,256]{1,2,0:T(8,128)} %get-tuple-element.93) | data formatting | bytes 6291456
  199.3 2.4 gather_fusion.3
  202.6 2.0 gather_fusion.2
  207.1 22.9 %all-reduce.3 = (f32[6,512]{1,0:T(8,128)}, f32[144]{0:T(256)}) all-reduce(f32[6,512]{1,0:T(8,128)S(1)} %get-tuple-element.92, f32[144]{0:T(256)S(1)} %multiply_reduce_fusion.4), channel_id=1, replica_groups=mesh['ep'=4,'tp'=8] {'tp'}, use_global_device_ids=true, to_apply=%region_19.20 | all-reduce | flops 3216 | bytes 25728 | tf_op jit(solution)/shard_map/psum | solution.py:108
  232.0 12.7 %all-reduce.5 = (f32[256]{0:T(256)}, f32[256]{0:T(256)}) all-reduce(f32[256]{0:T(256)S(1)} %multiply_reduce_fusion.6, f32[256]{0:T(256)S(1)} %multiply_reduce_fusion.5), channel_id=1, replica_groups=mesh['ep'=4,'tp'=8] {'ep'}, use_global_device_ids=true, to_apply=%region_21.22 | all-reduce | flops 512 | bytes 4096 | tf_op jit(solution)/shard_map/psum | solution.py:115
  (97 shorter events, 19.4 us)
Async XLA Ops:
  7.2 43.2 %copy-start = (bf16[6,256,512]{2,1,0:T(8,128)(2,1)S(1)}, bf16[6,256,512]{2,1,0:T(8,128)(2,1)}, u32[]{:S(2)}) copy-start(bf16[6,256,512]{2,1,0:T(8,128)(2,1)} %param.14) | copy-start | bytes 4718596
  9.7 17.1 %copy-start.3 = (bf16[160,256]{1,0:T(8,128)(2,1)S(1)}, bf16[160,256]{1,0:T(8,128)(2,1)}, u32[]{:S(2)}) copy-start(bf16[160,256]{1,0:T(8,128)(2,1)} %param.10) | copy-start | bytes 245764
  26.8 9.3 %copy-start.9 = (bf16[256,576]{0,1:T(8,128)(2,1)S(1)}, bf16[256,576]{0,1:T(8,128)(2,1)}, u32[]{:S(2)}) copy-start(bf16[256,576]{0,1:T(8,128)(2,1)} %param.18) | copy-start | bytes 884740
  26.9 10.1 %copy-start.14 = (bf16[160,256]{1,0:T(8,128)(2,1)S(1)}, bf16[160,256]{1,0:T(8,128)(2,1)}, u32[]{:S(2)}) copy-start(bf16[160,256]{1,0:T(8,128)(2,1)} %param.11) | copy-start | bytes 245764
  26.9 10.1 %copy-start.15 = (bf16[576,256]{1,0:T(8,128)(2,1)S(1)}, bf16[576,256]{1,0:T(8,128)(2,1)}, u32[]{:S(2)}) copy-start(bf16[576,256]{1,0:T(8,128)(2,1)} %param.19) | copy-start | bytes 884740
  29.7 13.9 %all-to-all-start.2 = ((bf16[14,24,256]{2,0,1:T(8,128)(2,1)}), bf16[14,24,256]{2,0,1:T(8,128)(2,1)S(1)}, u32[]{:S(2)}, u32[]{:S(2)}) async-start(bf16[14,24,256]{2,0,1:T(8,128)(2,1)} %copy.65), calls=%async_computation.2 | async-start | bytes 393216 | tf_op jit(solution)/shard_map/all_to_all | solution.py:62
  37.0 3.8 %copy-start.11 = (bf16[256,576]{0,1:T(8,128)(2,1)S(1)}, bf16[256,576]{0,1:T(8,128)(2,1)}, u32[]{:S(2)}) copy-start(bf16[256,576]{0,1:T(8,128)(2,1)} %param.17) | copy-start | bytes 884740
  43.5 4.1 %copy-start.13 = (bf16[14,24,256]{2,0,1:T(8,128)(2,1)}, bf16[14,24,256]{2,0,1:T(8,128)(2,1)S(1)}, u32[]{:S(2)}) copy-start(bf16[14,24,256]{2,0,1:T(8,128)(2,1)S(1)} %all-to-all-done.2) | copy-start | bytes 516100
  43.5 10.3 %all-to-all-start.1 = ((bf16[14,24,256]{2,0,1:T(8,128)(2,1)}), bf16[14,24,256]{2,0,1:T(8,128)(2,1)}, u32[]{:S(2)}, u32[]{:S(2)}) async-start(bf16[14,24,256]{2,0,1:T(8,128)(2,1)} %copy.63), calls=%async_computation.1 | async-start | bytes 393216 | tf_op jit(solution)/shard_map/all_to_all | solution.py:63
  47.5 85.1 %all-reduce.8.cloned.1.call-start = ((), (), s32[]{:S(2)}) async-start(), calls=%async_computation.11 | async-start | bytes 6586368 | tf_op jit(solution)/shard_map/psum | solution.py:74
  47.6 4.0 %copy-start.1 = (bf16[6,256,512]{2,1,0:T(8,128)(2,1)S(1)}, bf16[6,256,512]{2,1,0:T(8,128)(2,1)}, u32[]{:S(2)}) copy-start(bf16[6,256,512]{2,1,0:T(8,128)(2,1)} %param.15) | copy-start | bytes 4718596
  60.1 74.8 %copy-start.16 = (f32[160,2]{0,1:T(2,128)S(1)}, f32[160,2]{0,1:T(2,128)}, u32[]{:S(2)}) copy-start(f32[160,2]{0,1:T(2,128)} %param.13) | copy-start | bytes 3844
  60.1 146.0 %reduce-scatter.8.cloned.1.call-start = ((), (), s32[]{:S(2)}) async-start(), calls=%async_computation.10 | async-start | bytes 737280 | tf_op jit(solution)/shard_map/reduce_scatter | solution.py:100
  152.9 10.2 %all-to-all-start = ((f32[14,4,6]{0,2,1:T(8,128)}), f32[14,4,6]{0,2,1:T(8,128)S(1)}, u32[]{:S(2)}, u32[]{:S(2)}) async-start(f32[14,4,6]{0,2,1:T(8,128)} %all_to_all.61), calls=%async_computation | async-start | bytes 32768 | tf_op jit(solution)/shard_map/all_to_all | solution.py:65
  157.5 72.6 %reduce-scatter.6.cloned.1.call-start = ((), (), s32[]{:S(2)}) async-start(), calls=%async_computation.9 | async-start | bytes 737280 | tf_op jit(solution)/shard_map/reduce_scatter | solution.py:99
  165.3 0.7 copy-start.4
  170.7 15.6 %all-to-all-start.4 = ((f32[4,14,6]{1,2,0:T(8,128)}), f32[4,14,6]{1,2,0:T(8,128)S(1)}, u32[]{:S(2)}, u32[]{:S(2)}) async-start(f32[4,14,6]{1,2,0:T(8,128)} %copy.70), calls=%async_computation.4 | async-start | bytes 32768 | tf_op jit(solution)/shard_map/all_to_all | solution.py:89
  174.0 57.1 %reduce-scatter.4.cloned.1.call-start = ((), (), s32[]{:S(2)}) async-start(), calls=%async_computation.8 | async-start | bytes 737280 | tf_op jit(solution)/shard_map/reduce_scatter | solution.py:98
  176.0 2.4 copy-start.2
  178.4 2.9 %copy-start.7 = (bf16[56,6,256]{2,0,1:T(8,128)(2,1)S(1)}, bf16[56,6,256]{2,0,1:T(8,128)(2,1)}, u32[]{:S(2)}) copy-start(bf16[56,6,256]{2,0,1:T(8,128)(2,1)} %all_to_all.67) | copy-start | bytes 516100
  178.4 2.9 %copy-start.8 = (bf16[56,6,512]{2,0,1:T(8,128)(2,1)S(1)}, bf16[56,6,512]{2,0,1:T(8,128)(2,1)}, u32[]{:S(2)}) copy-start(bf16[56,6,512]{2,0,1:T(8,128)(2,1)} %get-tuple-element.83) | copy-start | bytes 1032196
  186.3 16.2 %all-to-all-start.3 = ((bf16[56,6,256]{2,1,0:T(8,128)(2,1)}), bf16[56,6,256]{2,1,0:T(8,128)(2,1)S(1)}, u32[]{:S(2)}, u32[]{:S(2)}) async-start(bf16[56,6,256]{2,1,0:T(8,128)(2,1)} %copy.67), calls=%async_computation.3 | async-start | bytes 458752 | tf_op jit(solution)/shard_map/all_to_all | solution.py:88
  195.2 3.6 %copy-start.6 = (bf16[160,576]{1,0:T(8,128)(2,1)S(1)}, bf16[160,576]{1,0:T(8,128)(2,1)}, u32[]{:S(2)}) copy-start(bf16[160,576]{1,0:T(8,128)(2,1)} %get-tuple-element.87) | copy-start | bytes 552964
  195.2 3.6 %copy-start.12 = (bf16[256,576]{0,1:T(8,128)(2,1)S(1)}, bf16[256,576]{0,1:T(8,128)(2,1)}, u32[]{:S(2)}) copy-start(bf16[256,576]{0,1:T(8,128)(2,1)} %param.17) | copy-start | bytes 884740
  202.5 2.7 %copy-start.5 = (bf16[160,576]{1,0:T(8,128)(2,1)S(1)}, bf16[160,576]{1,0:T(8,128)(2,1)}, u32[]{:S(2)}) copy-start(bf16[160,576]{1,0:T(8,128)(2,1)} %copy-done.4) | copy-start | bytes 552964
  202.5 2.7 %copy-start.10 = (bf16[256,576]{0,1:T(8,128)(2,1)S(1)}, bf16[256,576]{0,1:T(8,128)(2,1)}, u32[]{:S(2)}) copy-start(bf16[256,576]{0,1:T(8,128)(2,1)} %param.18) | copy-start | bytes 884740
Sparse Core Ops, SparseCore 0:
  60.2 72.3 all-reduce.7
  135.5 22.1 reduce-scatter.7
  167.2 19.7 reduce-scatter.5
  189.7 21.0 reduce-scatter.3
where the time goes:
time: 252 us; the launch traced here: 251 us
  waiting for transfers between devices  80.8 us (32%)
  local copies, waits for them, and re-layouts  59.6 us (24%)
  blocking collectives  35.7 us (14%)
  matrix products  28.3 us (11%)
  starting transfers between devices  23.3 us (9%)
  between operations  14.1 us (6%)
  other arithmetic  9.43 us (4%)
    psum x1, waiting for transfers between devices, per_device(): lax.psum((gate_part, up_part, back_part, s_gate_part, s_up_part, s_back_p...  72.4 us
    psum x1, blocking collectives, per_device(): lax.psum((jnp.sum(down_grad * down_grad, axis=2), jnp.sum(shared_down_gra...  22.9 us
    scatter x2, local copies, waits for them, and re-layouts, per_device(): slot_weight = jnp.zeros((capacity, experts_all), jnp.float32).at[slot_ran...  17.1 us
    scatter x1, local copies, waits for them, and re-layouts, per_device(): jnp.full((capacity, experts_all), tok_rows, jnp.int32).at[slot_rank, owners]  17 us
    psum x1, blocking collectives, per_device(): lax.psum((jnp.sum(shared_gate_grad * shared_gate_grad, axis=1), jnp.sum(s...  12.7 us
    all_to_all x1, starting transfers between devices, per_device(): lax.all_to_all(sent_x, 'ep', split_axis=1, concat_axis=0, tiled=True)  6.35 us
    unnamed x38, local copies, waits for them, and re-layouts  6.04 us
    all_to_all x1, waiting for transfers between devices, per_device(): lax.all_to_all(slot_weight, 'ep', split_axis=1, concat_axis=0, tiled=True)  5.6 us
  transfers between devices with their start and end apart: 9, of which 4 were waited for; matrix products, arithmetic and copies ran while one was open for 25% of the time, Pallas kernels for 0%

commit v1 on v0

v1 whole, which is shorter than its diff:
```python
import functools

import jax
import jax.numpy as jnp
from jax import lax
from jax.experimental import pallas as pl
from jax.experimental.pallas import tpu as pltpu
from jax.sharding import PartitionSpec as P

BF = jnp.bfloat16
F32 = jnp.float32
MESH = pl.DeviceIdType.MESH
VMEM = pl.BlockSpec(memory_space=pltpu.VMEM)


def up_to(value, unit):
    return (value + unit - 1) // unit * unit


def silu_parts(pre):
    logistic = jax.nn.sigmoid(pre)
    return (pre * logistic, logistic * (1.0 + pre * (1.0 - logistic)))


def remote(src, dst, send, recv, where):
    return pltpu.make_async_remote_copy(
        src_ref=src,
        dst_ref=dst,
        send_sem=send,
        recv_sem=recv,
        device_id=where,
        device_id_type=MESH,
    )


def greet(places):
    barrier = pltpu.get_barrier_semaphore()
    for place in places:
        pl.semaphore_signal(barrier, inc=1, device_id=place, device_id_type=MESH)
    pl.semaphore_wait(barrier, len(places))


def gather_kernel(n_ep, x, dy, meta, all_x, all_dy, all_meta, send, recv):
    me = lax.axis_index("ep")
    peers = [lax.rem(me + d, n_ep) for d in range(1, n_ep)]
    greet([{"ep": p} for p in peers])
    pairs = ((meta, all_meta), (x, all_x), (dy, all_dy))
    copies = []
    for d, p in enumerate(peers):
        for k, (src, dst) in enumerate(pairs):
            c = remote(src, dst.at[me], send.at[d, k], recv.at[d, k], {"ep": p})
            c.start()
            copies.append(c)
    for src, dst in pairs:
        dst[me] = src[...]
    for c in copies:
        c.wait()


def hidden_kernel(
    n_tp, cols, g, u, b, s, rw, hid, gg, gu, so, dots,
    pg, pu, pb, ps, hg, hu, hb, hs, cg, cu, cb, cs,
    a_send, a_recv, b_send, b_recv, c_send, c_recv, d_send, d_recv,
):
    me = lax.axis_index("tp")
    half = n_tp // 2
    parity = lax.rem(me, 2)
    mine = me // 2
    partner = {"tp": me + 1 - 2 * parity}
    others = [lax.rem(mine + d, half) for d in range(1, half)]
    places = [{"tp": 2 * j + parity} for j in others]
    rows = g.shape[0] // n_tp
    s_rows = s.shape[0] // n_tp
    greet([partner] + places)

    full = (s, g, u, b)
    got = (ps, pg, pu, pb)
    held = (hs, hg, hu, hb)
    landed = (cs, cg, cu, cb)
    sizes = (s_rows, rows, rows, rows)

    def span(start, size):
        return pl.ds(pl.multiple_of(start * size, size), size)

    first = []
    for k in range(4):
        c = remote(
            full[k].at[span(1 - parity, half * sizes[k])],
            got[k],
            a_send.at[k],
            a_recv.at[k],
            partner,
        )
        c.start()
        first.append(c)
    second = []
    for k in range(4):
        first[k].wait()
        held[k][...] = (
            full[k][span(parity, half * sizes[k]), :].astype(F32) + got[k][...].astype(F32)
        ).astype(BF)
        for d, j in enumerate(others):
            c = remote(
                held[k].at[span(j, sizes[k])],
                landed[k].at[d],
                b_send.at[d, k],
                b_recv.at[d, k],
                places[d],
            )
            c.start()
            second.append(c)

    place = parity * half + mine

    def total(k):
        for d in range(half - 1):
            second[k * (half - 1) + d].wait_recv()
        out = full[k][span(place, sizes[k]), :].astype(F32)
        out = out + got[k][span(mine, sizes[k]), :].astype(F32)
        for d in range(half - 1):
            out = out + landed[k][d].astype(F32)
        return out

    last = []

    def share(k, ref, where):
        block = ref.at[where]
        c = remote(block, block, d_send.at[0, k], d_recv.at[0, k], partner)
        c.start()
        last.append(c)
        for d in range(half - 1):
            c = remote(block, block, c_send.at[d, k], c_recv.at[d, k], places[d])
            c.start()
            last.append(c)

    both = total(0)
    width = both.shape[1]
    lane = lax.broadcasted_iota(jnp.int32, both.shape, 1)
    s_up = pltpu.roll(both, width - cols, 1)
    s_back = pltpu.roll(both, width - 2 * cols, 1)
    s_out, s_slope = silu_parts(both)
    s_hidden = s_out * s_up
    s_dgate = pltpu.roll(s_back * s_up * s_slope, cols, 1)
    s_dup = pltpu.roll(s_back * s_out, 2 * cols, 1)
    so[span(place, s_rows), :] = jnp.where(
        lane < cols, s_hidden, jnp.where(lane < 2 * cols, s_dgate, s_dup)
    ).astype(BF)
    share(0, so, span(place, s_rows))

    gate, up, back = total(1), total(2), total(3)
    silu_out, silu_slope = silu_parts(gate)
    hidden = (silu_out * up).astype(BF)
    dhidden = rw[span(place, rows), :][:, :1] * back
    mine_rows = span(place, rows)
    hid[mine_rows, :] = hidden
    gg[mine_rows, :] = (dhidden * up * silu_slope).astype(BF)
    gu[mine_rows, :] = (dhidden * silu_out).astype(BF)
    dots[place] = lax.dot_general(
        jnp.ones((8, gate.shape[1]), F32),
        hidden.astype(F32) * back,
        (((1,), (1,)), ((), ())),
        precision=lax.Precision.HIGHEST,
        preferred_element_type=F32,
    )
    outs = ((so, s_rows), (hid, rows), (gg, rows), (gu, rows), (dots, 1))
    for k in range(1, 4):
        share(k, outs[k][0], mine_rows)
    share(4, dots, pl.ds(place, 1))

    for k, (ref, size) in enumerate(outs):
        for d in range(half - 1):
            source = lax.rem(mine + half - 1 - d, half)
            at = parity * half + source
            where = pl.ds(at, 1) if k == 4 else span(at, size)
            block = ref.at[where]
            remote(
                block, block, c_send.at[d, k], c_recv.at[d, k], places[d]
            ).wait_recv()
            c = remote(block, block, d_send.at[1 + d, k], d_recv.at[1 + d, k], partner)
            c.start()
            last.append(c)
    for c in second:
        c.wait_send()
    for k, (ref, size) in enumerate(outs):
        for d in range(half):
            source = mine if d == 0 else lax.rem(mine + half - d, half)
            at = (1 - parity) * half + source
            where = pl.ds(at, 1) if k == 4 else span(at, size)
            block = ref.at[where]
            remote(block, block, d_send.at[d, k], d_recv.at[d, k], partner).wait_recv()
    for c in last:
        c.wait_send()


def finish_kernel(
    n_ep, n_tp, tg, wg, es, ts, token_out, wg_out, es_out, ts_out,
    tg_in, wg_in, es_in, ts_in, e_send, e_recv, t_send, t_recv,
):
    ep, tp = lax.axis_index("ep"), lax.axis_index("tp")
    eps = [lax.rem(ep + d, n_ep) for d in range(1, n_ep)]
    tps = [lax.rem(tp + d, n_tp) for d in range(1, n_tp)]
    greet([{"ep": p} for p in eps] + [{"tp": p} for p in tps])
    copies = []
    for d, p in enumerate(eps):
        for k, (src, dst) in enumerate(
            ((tg.at[p], tg_in.at[d]), (wg.at[p], wg_in.at[d]), (es, es_in.at[d]))
        ):
            copies.append(remote(src, dst, e_send.at[d, k], e_recv.at[d, k], {"ep": p}))
            copies[-1].start()
    for d, p in enumerate(tps):
        copies.append(remote(ts, ts_in.at[d], t_send.at[d], t_recv.at[d], {"tp": p}))
        copies[-1].start()
    for c in copies:
        c.wait()
    rows = tg[ep].astype(F32)
    weights = wg[ep]
    norms = es[...]
    for d in range(n_ep - 1):
        rows = rows + tg_in[d].astype(F32)
        weights = weights + wg_in[d]
        norms = norms + es_in[d]
    token_out[...] = rows.astype(BF)
    wg_out[...] = weights
    es_out[...] = norms
    down = ts[...]
    for d in range(n_tp - 1):
        down = down + ts_in[d]
    ts_out[...] = down


def call(kernel, collective, outs, scratch, *args):
    return pl.pallas_call(
        kernel,
        out_shape=[jax.ShapeDtypeStruct(s, t) for s, t in outs],
        in_specs=[VMEM] * len(args),
        out_specs=[VMEM] * len(outs),
        scratch_shapes=scratch,
        compiler_params=pltpu.CompilerParams(
            collective_id=collective,
            has_side_effects=True,
            vmem_limit_bytes=48 * 1024 * 1024,
        ),
    )(*args)


def per_device(
    n_ep, n_tp,
    tokens, cotangent, routes, gate_weights,
    expert_gate, expert_up, expert_down,
    shared_gate, shared_up, shared_down,
):
    dma = pltpu.SemaphoreType.DMA
    half = n_tp // 2
    tok_rows, narrow = tokens.shape
    picks = routes.shape[1]
    experts, _, ff = expert_gate.shape
    experts_all = experts * n_ep
    capacity = max(2, (tok_rows * picks + experts_all - 1) // experts_all)
    every = tok_rows * n_ep
    sf = shared_gate.shape[1]
    cols = sf // n_ep
    ep = lax.axis_index("ep")

    meta = jnp.concatenate([routes.astype(F32), gate_weights], axis=1).T
    meta = jnp.pad(meta, ((0, up_to(2 * picks, 8) - 2 * picks), (0, 0)))
    all_x, all_dy, all_meta = call(
        functools.partial(gather_kernel, n_ep),
        0,
        [
            ((n_ep, tok_rows, narrow), BF),
            ((n_ep, tok_rows, narrow), BF),
            ((n_ep,) + meta.shape, F32),
        ],
        [dma((n_ep - 1, 3)), dma((n_ep - 1, 3))],
        tokens, cotangent, meta,
    )
    all_x = all_x.reshape(every, narrow)
    all_dy = all_dy.reshape(every, narrow)

    ids = (ep * experts + jnp.arange(experts, dtype=jnp.int32)).astype(F32)
    match = all_meta[:, :picks, None, :] == ids[None, None, :, None]
    chosen = jnp.any(match, axis=1)
    weight_of = jnp.sum(
        jnp.where(match, all_meta[:, picks : 2 * picks, None, :], 0.0), axis=1
    )
    before = jnp.triu(jnp.ones((tok_rows, tok_rows), BF), 1)
    rank = jnp.einsum(
        "bet,ts->bes", chosen.astype(BF), before, preferred_element_type=F32
    ).astype(jnp.int32)
    slot = jnp.where(
        chosen,
        rank + capacity * jnp.arange(n_ep, dtype=jnp.int32)[:, None, None],
        -1,
    )
    per_expert = up_to(capacity * n_ep, 16)
    used = experts * per_expert
    rows = up_to(used, 16 * n_tp)
    slot = slot.transpose(1, 0, 2).reshape(experts, 1, every)
    hot = slot == jnp.arange(per_expert, dtype=jnp.int32)[None, :, None]
    onehot = hot.astype(BF)
    row_weight = jnp.sum(
        jnp.where(hot, weight_of.transpose(1, 0, 2).reshape(experts, 1, every), 0.0), axis=2
    )
    recv_x = jnp.einsum("ert,tl->erl", onehot, all_x, preferred_element_type=BF)
    recv_dy = jnp.einsum("ert,tl->erl", onehot, all_dy, preferred_element_type=BF)

    def flat(a):
        return jnp.pad(a.reshape(used, a.shape[-1]), ((0, rows - used), (0, 0)))

    gate_part = flat(jnp.einsum("erl,elf->erf", recv_x, expert_gate, preferred_element_type=BF))
    up_part = flat(jnp.einsum("erl,elf->erf", recv_x, expert_up, preferred_element_type=BF))
    back_part = flat(jnp.einsum("erl,efl->erf", recv_dy, expert_down, preferred_element_type=BF))
    s_pair = jnp.concatenate(
        [
            lax.dynamic_slice_in_dim(shared_gate, ep * cols, cols, 1),
            lax.dynamic_slice_in_dim(shared_up, ep * cols, cols, 1),
        ],
        axis=1,
    )
    s_down = lax.dynamic_slice_in_dim(shared_down, ep * cols, cols, 0)
    width = up_to(3 * cols, 128)
    s_part = jnp.concatenate(
        [
            jnp.dot(all_x, s_pair, preferred_element_type=BF),
            jnp.einsum("tl,sl->ts", all_dy, s_down, preferred_element_type=BF),
            jnp.zeros((every, width - 3 * cols), BF),
        ],
        axis=1,
    )
    row_weight_wide = jnp.broadcast_to(flat(row_weight[:, :, None]), (rows, 128))
    chunk, s_chunk = rows // n_tp, every // n_tp
    hidden, grad_gate, grad_up, s_all, dots = call(
        functools.partial(hidden_kernel, n_tp, cols),
        1,
        [
            ((rows, ff), BF),
            ((rows, ff), BF),
            ((rows, ff), BF),
            ((every, width), BF),
            ((n_tp, 8, chunk), F32),
        ],
        [pltpu.VMEM((rows // 2, ff), BF)] * 3
        + [pltpu.VMEM((every // 2, width), BF)]
        + [pltpu.VMEM((rows // 2, ff), BF)] * 3
        + [pltpu.VMEM((every // 2, width), BF)]
        + [pltpu.VMEM((half - 1, chunk, ff), BF)] * 3
        + [pltpu.VMEM((half - 1, s_chunk, width), BF)]
        + [
            dma((4,)), dma((4,)), dma((half - 1, 4)), dma((half - 1, 4)),
            dma((half - 1, 5)), dma((half - 1, 5)), dma((half, 5)), dma((half, 5)),
        ],
        gate_part, up_part, back_part, s_part, row_weight_wide,
    )
    hidden = hidden[:used].reshape(experts, per_expert, ff)
    grad_gate = grad_gate[:used].reshape(experts, per_expert, ff)
    grad_up = grad_up[:used].reshape(experts, per_expert, ff)
    dots = dots[:, 0, :].reshape(rows)[:used].reshape(experts, per_expert)

    weighted = (row_weight[:, :, None] * recv_dy.astype(F32)).astype(BF)
    down_grad = jnp.einsum("erf,erl->efl", hidden, weighted, preferred_element_type=F32)
    gate_wgrad = jnp.einsum("erl,erf->elf", recv_x, grad_gate, preferred_element_type=F32)
    up_wgrad = jnp.einsum("erl,erf->elf", recv_x, grad_up, preferred_element_type=F32)
    row_grad = (
        jnp.einsum("erf,elf->erl", grad_gate, expert_gate, preferred_element_type=F32)
        + jnp.einsum("erf,elf->erl", grad_up, expert_up, preferred_element_type=F32)
    ).astype(BF)
    s_hidden = s_all[:, :cols]
    s_grads = s_all[:, cols : 3 * cols]
    shared_pair = jnp.einsum("tl,ts->ls", all_x, s_grads, preferred_element_type=F32)
    shared_gate_grad, shared_up_grad = shared_pair[:, :cols], shared_pair[:, cols:]
    shared_down_grad = jnp.einsum("ts,tl->sl", s_hidden, all_dy, preferred_element_type=F32)
    token_part = (
        jnp.einsum("ert,erl->tl", onehot, row_grad, preferred_element_type=F32)
        + jnp.einsum("ts,ls->tl", s_grads, s_pair, preferred_element_type=F32)
    ).astype(BF)
    dot_of = jnp.sum(jnp.where(hot, dots[:, :, None], 0.0), axis=1)
    dot_of = dot_of.reshape(experts, n_ep, tok_rows).transpose(1, 0, 2)
    weight_part = jnp.sum(jnp.where(match, dot_of[:, None], 0.0), axis=2)
    weight_part = jnp.pad(weight_part, ((0, 0), (0, up_to(picks, 8) - picks), (0, 0)))
    gate_rows_sq = jnp.sum(gate_wgrad * gate_wgrad, axis=2)
    up_rows_sq = jnp.sum(up_wgrad * up_wgrad, axis=2)
    down_sq = jnp.sum(down_grad * down_grad, axis=2)
    shared_down_sq = jnp.sum(shared_down_grad * shared_down_grad, axis=1)
    over_tp = jnp.concatenate(
        [down_sq, jnp.pad(shared_down_sq, (0, ff - cols))[None]], axis=0
    )
    over_tp = jnp.pad(over_tp, ((0, up_to(experts + 1, 8) - experts - 1), (0, 0)))
    over_ep = jnp.stack(
        [
            jnp.sum(shared_gate_grad * shared_gate_grad, axis=1),
            jnp.sum(shared_up_grad * shared_up_grad, axis=1),
        ]
    )
    over_ep = jnp.pad(over_ep, ((0, 6), (0, 0)))
    peers, t_peers = n_ep - 1, n_tp - 1
    token_grad, weight_grad, over_ep, over_tp = call(
        functools.partial(finish_kernel, n_ep, n_tp),
        2,
        [
            ((tok_rows, narrow), BF),
            (weight_part.shape[1:], F32),
            (over_ep.shape, F32),
            (over_tp.shape, F32),
        ],
        [
            pltpu.VMEM((peers, tok_rows, narrow), BF),
            pltpu.VMEM((peers,) + weight_part.shape[1:], F32),
            pltpu.VMEM((peers,) + over_ep.shape, F32),
            pltpu.VMEM((t_peers,) + over_tp.shape, F32),
            dma((peers, 3)), dma((peers, 3)), dma((t_peers,)), dma((t_peers,)),
        ],
        token_part.reshape(n_ep, tok_rows, narrow), weight_part, over_ep, over_tp,
    )
    return (
        token_grad,
        weight_grad[:picks].T,
        gate_wgrad,
        up_wgrad,
        down_grad,
        shared_gate_grad,
        shared_up_grad,
        shared_down_grad,
        gate_rows_sq,
        up_rows_sq,
        over_tp[:experts],
        over_ep[0],
        over_ep[1],
        over_tp[experts, :cols],
    )


def solution(mesh):
    n_ep, n_tp = mesh.shape["ep"], mesh.shape["tp"]
    return jax.shard_map(
        functools.partial(per_device, n_ep, n_tp),
        mesh=mesh,
        in_specs=(
            P("ep", "tp"),
            P("ep", "tp"),
            P("ep", None),
            P("ep", None),
            P("ep", "tp", None),
            P("ep", "tp", None),
            P("ep", None, "tp"),
            P("tp", None),
            P("tp", None),
            P(None, "tp"),
        ),
        out_specs=(
            P("ep", "tp"),
            P("ep", None),
            P("ep", "tp", None),
            P("ep", "tp", None),
            P("ep", None, "tp"),
            P("tp", "ep"),
            P("tp", "ep"),
            P("ep", "tp"),
            P("ep", "tp"),
            P("ep", "tp"),
            P("ep", None),
            P("tp"),
            P("tp"),
            P("ep"),
        ),
        check_vma=False,
    )
```

time: 252 us -> 99.7 us (0.40)
  waiting for transfers between devices: 80.8 us -> 0 us
  Pallas kernels: 0 us -> 59.4 us
  local copies, waits for them, and re-layouts: 59.6 us -> 10.8 us
  blocking collectives: 35.7 us -> 0 us
  starting transfers between devices: 23.3 us -> 0 us
  between operations: 14.1 us -> 0.94 us
  other arithmetic: 9.43 us -> 4.51 us
  matrix products: 28.3 us -> 23.4 us
    psum x1 -> x0, waiting for transfers between devices: 72.4 us -> none  [per_device(): lax.psum((gate_part, up_part, back_part, s_gate_part, s_up_part, s_back_p...]
    pallas_call x0 -> x3, Pallas kernels: none -> 59.4 us  [call(): pl.pallas_call(kernel, out_shape=[jax.ShapeDtypeStruct(s, t) for s, t in...]
    psum x2 -> x0, blocking collectives: 35.7 us -> none  [the longest x1 22.9 us: per_device(): lax.psum((jnp.sum(down_grad * down_grad, axis=2), jnp.sum(shared_down_gra...]
    scatter x3 -> x0, local copies, waits for them, and re-layouts: 34.1 us -> none  [the longest x2 17.1 us: per_device(): slot_weight = jnp.zeros((capacity, experts_all), jnp.float32).at[slot_ran...]
    all_to_all x5 -> x0, starting transfers between devices: 23.2 us -> none  [the longest x1 6.35 us: per_device(): lax.all_to_all(sent_x, 'ep', split_axis=1, concat_axis=0, tiled=True)]
    gather x6 -> x0, local copies, waits for them, and re-layouts: 9.93 us -> none  [the longest x2 2.74 us: per_device(): sent_x = jnp.concatenate([tokens, zero_row], axis=0)[slot_tok]]
    all_to_all x5 -> x0, waiting for transfers between devices: 8.32 us -> none  [the longest x1 5.6 us: per_device(): lax.all_to_all(slot_weight, 'ep', split_axis=1, concat_axis=0, tiled=True)]
    all_to_all x10 -> x0, local copies, waits for them, and re-layouts: 7.44 us -> none  [the longest x2 3.29 us: per_device(): lax.all_to_all(sent_dy, 'ep', split_axis=1, concat_axis=0, tiled=True)]
  transfers between devices with their start and end apart: 9 -> 0, of which waited for: 4 -> 0; matrix products, arithmetic and copies ran while one was open for 25% -> 0% of each run, Pallas kernels for 0% -> 0%
where the time goes in v1:
time: 99.7 us; the launch traced here: 99.1 us
  Pallas kernels  59.4 us (60%)
  matrix products  23.4 us (23%)
  local copies, waits for them, and re-layouts  10.8 us (11%)
  other arithmetic  4.51 us (5%)
    pallas_call x3, Pallas kernels, call(): pl.pallas_call(kernel, out_shape=[jax.ShapeDtypeStruct(s, t) for s, t in...  59.4 us
    unnamed x25, local copies, waits for them, and re-layouts  7.29 us
    dot_general x1, matrix products, per_device(): jnp.einsum('erf,erl->efl', hidden, weighted, preferred_element_type=F32)  3.1 us
    dot_general x1, matrix products, per_device(): jnp.einsum('erl,erf->elf', recv_x, grad_gate, preferred_element_type=F32)  2.89 us
    dot_general x1, matrix products, per_device(): jnp.einsum('erl,erf->elf', recv_x, grad_up, preferred_element_type=F32)  2.88 us
    dot_general x1, matrix products, per_device(): jnp.einsum('erf,elf->erl', grad_gate, expert_gate, preferred_element_type...  2.75 us
    dot_general x1, matrix products, per_device(): jnp.einsum('ert,erl->tl', onehot, row_grad, preferred_element_type=F32)  2.73 us

profile of v1, /device:TPU:0, one launch (start us, length us, event | category | flops | bytes accessed | tf_op | source)
XLA Modules:
  0.0 99.1 jit_solution(9329026089612411612)
XLA Ops:
  0.7 1.1 %constant_dynamic-slice_fusion = (bf16[256,144]{0,1:T(8,128)(2,1)S(1)}, bf16[256,144]{0,1:T(8,128)(2,1)S(1)}) fusion(bf16[256,576]{0,1:T(8,128)(2,1)} %param.18, s32[]{:T(128)S(6)} %select_n.36, bf16[256,576]{0,1:T(8,128)(2,1)} %param.17), kind=kLoop, calls=%fused_computation.55 | loop fusion | bytes 294916 | tf_op jit(solution)/shard_map/dynamic_slice | solution.py:316
  1.7 0.7 convert_element_type.39
  2.4 0.7 maximum_bitcast_fusion
  3.1 0.9 copy-done.4
  4.0 0.9 copy-done.5
  4.9 17.3 %shard_map.209 = (bf16[4,160,256]{2,1,0:T(8,128)(2,1)S(1)}, bf16[4,160,256]{2,1,0:T(8,128)(2,1)S(1)}, f32[4,8,160]{2,1,0:T(8,128)S(1)}) custom-call(bf16[160,256]{1,0:T(8,128)(2,1)S(1)} %copy-done.4, bf16[160,256]{1,0:T(8,128)(2,1)S(1)} %copy-done.5, f32[8,160]{1,0:T(8,128)S(1)} %pad.20.meta), custom_call_target="tpu_custom_call" | custom-call | tf_op jit(solution)/shard_map/pallas_call | solution.py:232
  22.2 0.4 fusion.18
  22.6 1.1 %fusion.21 = bf16[640,144]{1,0:T(8,128)(2,1)S(1)} fusion(bf16[640,256]{1,0:T(8,128)(2,1)S(1)} %bitcast.66, bf16[576,256]{1,0:T(8,128)(2,1)} %param.19, s32[]{:T(128)S(6)} %select_n.36), kind=kOutput, calls=%fused_computation.37 | convolution fusion | flops 47185920 | bytes 585732 | tf_op jit(solution)/shard_map/tl,sl->ts/dot_general | solution.py:325
  25.0 0.3 fusion.6
  25.3 1.9 %fusion.35 = bf16[6,64,512]{2,1,0:T(8,128)(2,1)S(1)} fusion(bf16[6,64,256]{2,1,0:T(8,128)(2,1)S(1)} %fusion.6, bf16[6,256,512]{2,1,0:T(8,128)(2,1)} %param.14), kind=kOutput, calls=%fused_computation.65 | convolution fusion | flops 100663296 | bytes 2162688 | tf_op jit(solution)/shard_map/erl,elf->erf/dot_general | solution.py:310
  27.2 0.4 fusion.36
  28.0 0.6 copy-done.8
  28.6 0.6 fusion.37
  29.2 27.2 %shard_map.210 = (bf16[384,512]{1,0:T(8,128)(2,1)S(1)}, bf16[384,512]{1,0:T(8,128)(2,1)S(1)}, bf16[384,512]{1,0:T(8,128)(2,1)S(1)}, bf16[640,512]{1,0:T(8,128)(2,1)S(1)}, f32[8,8,48]{2,1,0:T(8,128)S(1)}) custom-call(bf16[384,512]{1,0:T(8,128)(2,1)S(1)} %bitcast.58, bf16[384,512]{1,0:T(8,128)(2,1)S(1)} %bitcast.59, bf16[384,512]{1,0:T(8,128)(2,1)S(1)} %bitcast.60, ...), custom_call_target="tpu_custom_call" | custom-call | tf_op jit(solution)/shard_map/pallas_call | solution.py:232
  56.4 3.1 %multiply_reduce_fusion.2 = (f32[6,512]{1,0:T(8,128)}, f32[6,512,256]{1,2,0:T(8,128)}) fusion(bf16[6,64,512]{2,1,0:T(8,128)(2,1)S(1)} %bitcast.65, bf16[6,64,256]{2,1,0:T(8,128)(2,1)S(1)} %fusion.5, f32[6,64]{1,0:T(8,128)S(1)} %select_reduce_fusion.1), kind=kOutput, calls=%fused_computation.2 | convolution fusion | flops 102528000 | bytes 3749376 | tf_op jit(solution)/shard_map/erf,erl->efl/dot_general | solution.py:360
  59.6 3.6 %copy.40 = f32[6,512,256]{2,1,0:T(8,128)} copy(f32[6,512,256]{1,2,0:T(8,128)} %get-tuple-element.93) | data formatting | bytes 6291456
  63.2 1.9 %multiply_reduce_fusion.3 = (f32[144]{0:T(256)S(1)}, f32[144,256]{1,0:T(8,128)}) fusion(bf16[640,256]{1,0:T(8,128)(2,1)} %bitcast.68, bf16[640,512]{1,0:T(8,128)(2,1)S(1)} %copy-done.2), kind=kOutput, calls=%fused_computation.32 | convolution fusion | flops 47259504 | bytes 803392 | tf_op jit(solution)/shard_map/ts,tl->sl/dot_general | solution.py:371
  65.1 0.7 select_maximum_fusion.ts
  65.8 0.6 fusion.10
  66.4 0.7 multiply_reduce_fusion.5
  67.2 1.0 select_reduce_fusion
  68.4 2.8 %fusion.38 = f32[6,64,256]{2,1,0:T(8,128)} fusion(bf16[6,64,512]{2,1,0:T(8,128)(2,1)S(1)} %bitcast.54, bf16[6,256,512]{2,1,0:T(8,128)(2,1)} %param.14), kind=kOutput, calls=%fused_computation.68 | convolution fusion | flops 100663296 | bytes 2359296 | tf_op jit(solution)/shard_map/erf,elf->erl/dot_general | solution.py:364
  71.2 2.7 %convolution_bitcast_fusion = f32[640,256]{1,0:T(8,128)} fusion(f32[6,64,256]{2,1,0:T(8,128)} %fusion.38, bf16[6,64,512]{2,1,0:T(8,128)(2,1)S(1)} %bitcast.56, bf16[6,256,512]{2,1,0:T(8,128)(2,1)S(1)} %copy-done, s32[6,640]{1,0:T(8,128)S(1)} %copy-done.10), kind=kOutput, calls=%fused_computation.4 | convolution fusion | flops 226934784 | bytes 3030016 | tf_op jit(solution)/shard_map/ert,erl->tl/dot_general | solution.py:373
  73.9 1.5 %fusion = bf16[640,256]{1,0:T(8,128)(2,1)S(1)} fusion(f32[640,256]{1,0:T(8,128)} %convolution_bitcast_fusion, bf16[640,512]{1,0:T(8,128)(2,1)S(1)} %copy-done.2, bf16[256,144]{0,1:T(8,128)(2,1)S(1)} %get-tuple-element.98, bf16[256,144]{0,1:T(8,128)(2,1)S(1)} %get-tuple-element.99), kind=kOutput, calls=%fused_computation.5 | convolution fusion | flops 94994432 | bytes 1622016 | tf_op jit(solution)/shard_map/ts,ls->tl/dot_general | solution.py:374
  75.4 14.9 %shard_map.211 = (bf16[160,256]{1,0:T(8,128)(2,1)S(1)}, f32[8,160]{1,0:T(8,128)S(1)}, f32[8,256]{1,0:T(8,128)S(1)}, f32[8,512]{1,0:T(8,128)S(1)}) custom-call(bf16[4,160,256]{2,1,0:T(8,128)(2,1)S(1)} %bitcast.61, f32[4,8,160]{2,1,0:T(8,128)S(1)} %pad.21.wg, f32[8,256]{1,0:T(8,128)S(1)} %select_maximum_fusion.1.es, f32[8,512]{1,0:T(8,128)S(1)} %select_maximum_fusion.ts), custom_call_target="tpu_custom_call" | custom-call | tf_op jit(solution)/shard_map/pallas_call | solution.py:232
  90.3 0.6 fusion.34
  90.9 0.6 slice_bitcast_fusion
  91.5 0.6 slice.47
  92.0 2.9 %multiply_reduce_fusion.1 = (f32[6,256]{1,0:T(8,128)}, f32[6,256,512]{2,1,0:T(8,128)}) fusion(bf16[6,64,256]{2,1,0:T(8,128)(2,1)S(1)} %copy-done.7, bf16[6,64,512]{2,1,0:T(8,128)(2,1)S(1)} %bitcast.55), kind=kOutput, calls=%fused_computation.1 | convolution fusion | flops 102234624 | bytes 3741696 | tf_op jit(solution)/shard_map/erl,erf->elf/dot_general | solution.py:361
  94.9 2.9 %multiply_reduce_fusion = (f32[6,256]{1,0:T(8,128)}, f32[6,256,512]{2,1,0:T(8,128)}) fusion(bf16[6,64,256]{2,1,0:T(8,128)(2,1)S(1)} %copy-done.7, bf16[6,64,512]{2,1,0:T(8,128)(2,1)S(1)} %bitcast.57), kind=kOutput, calls=%fused_computation | convolution fusion | flops 102234624 | bytes 3741696 | tf_op jit(solution)/shard_map/erl,erf->elf/dot_general | solution.py:362
  97.8 0.6 copy.47
  98.4 0.6 copy.48
  (46 shorter events, 1.9 us)
Async XLA Ops:
  0.6 26.6 %copy-start = (bf16[6,256,512]{2,1,0:T(8,128)(2,1)S(1)}, bf16[6,256,512]{2,1,0:T(8,128)(2,1)}, u32[]{:S(2)}) copy-start(bf16[6,256,512]{2,1,0:T(8,128)(2,1)} %param.15) | copy-start | bytes 4718596
  3.1 0.9 copy-start.4
  4.0 0.9 copy-start.5
  22.2 5.4 %copy-start.3 = (bf16[4,160,256]{2,1,0:T(8,128)(2,1)}, bf16[4,160,256]{2,1,0:T(8,128)(2,1)S(1)}, u32[]{:S(2)}) copy-start(bf16[4,160,256]{2,1,0:T(8,128)(2,1)S(1)} %get-tuple-element.28) | copy-start | bytes 983044
  24.4 3.2 %copy-start.9 = (s32[6,640]{1,0:T(8,128)}, s32[6,640]{1,0:T(8,128)S(1)}, u32[]{:S(2)}) copy-start(s32[6,640]{1,0:T(8,128)S(1)} %eq.31) | copy-start | bytes 46084
  25.3 2.3 %copy-start.6 = (bf16[6,64,256]{2,1,0:T(8,128)(2,1)}, bf16[6,64,256]{2,1,0:T(8,128)(2,1)S(1)}, u32[]{:S(2)}) copy-start(bf16[6,64,256]{2,1,0:T(8,128)(2,1)S(1)} %fusion.6) | copy-start | bytes 589828
  27.2 1.4 %copy-start.8 = (bf16[6,512,256]{2,1,0:T(8,128)(2,1)S(1)}, bf16[6,512,256]{2,1,0:T(8,128)(2,1)}, u32[]{:S(2)}) copy-start(bf16[6,512,256]{2,1,0:T(8,128)(2,1)} %param.16) | copy-start | bytes 4718596
  56.4 3.1 %copy-start.1 = (bf16[640,512]{1,0:T(8,128)(2,1)}, bf16[640,512]{1,0:T(8,128)(2,1)S(1)}, u32[]{:S(2)}) copy-start(bf16[640,512]{1,0:T(8,128)(2,1)S(1)} %get-tuple-element.31) | copy-start | bytes 1966084
  59.6 3.6 %copy-start.2 = (bf16[640,512]{1,0:T(8,128)(2,1)S(1)}, bf16[640,512]{1,0:T(8,128)(2,1)}, u32[]{:S(2)}) copy-start(bf16[640,512]{1,0:T(8,128)(2,1)} %copy-done.1) | copy-start | bytes 1966084
  66.4 4.8 %copy-start.10 = (s32[6,640]{1,0:T(8,128)S(1)}, s32[6,640]{1,0:T(8,128)}, u32[]{:S(2)}) copy-start(s32[6,640]{1,0:T(8,128)} %copy-done.9) | copy-start | bytes 46084
  73.9 18.1 %copy-start.7 = (bf16[6,64,256]{2,1,0:T(8,128)(2,1)S(1)}, bf16[6,64,256]{2,1,0:T(8,128)(2,1)}, u32[]{:S(2)}) copy-start(bf16[6,64,256]{2,1,0:T(8,128)(2,1)} %copy-done.6) | copy-start | bytes 589828

commit v2 on v1

v2 whole, which is shorter than its diff:
```python
import functools

import jax
import jax.numpy as jnp
from jax import lax
from jax.experimental import pallas as pl
from jax.experimental.pallas import tpu as pltpu
from jax.sharding import PartitionSpec as P

BF = jnp.bfloat16
F32 = jnp.float32
MESH = pl.DeviceIdType.MESH
VMEM = pl.BlockSpec(memory_space=pltpu.VMEM)


def up_to(value, unit):
    return (value + unit - 1) // unit * unit


def silu_parts(pre):
    logistic = jax.nn.sigmoid(pre)
    return (pre * logistic, logistic * (1.0 + pre * (1.0 - logistic)))


def remote(src, dst, send, recv, where):
    return pltpu.make_async_remote_copy(
        src_ref=src,
        dst_ref=dst,
        send_sem=send,
        recv_sem=recv,
        device_id=where,
        device_id_type=MESH,
    )


def greet(places):
    barrier = pltpu.get_barrier_semaphore()
    for place in places:
        pl.semaphore_signal(barrier, inc=1, device_id=place, device_id_type=MESH)
    pl.semaphore_wait(barrier, len(places))


def dot(left, right, left_dim, right_dim, precision=None):
    return lax.dot_general(
        left,
        right,
        (((left_dim,), (right_dim,)), ((), ())),
        precision=precision,
        preferred_element_type=F32,
    )


def front_kernel(
    n_ep, n_tp, experts, per_expert, capacity, picks, cols,
    x, dy, meta, w_gate, w_up, w_down, s_in, s_in_back, s_out_w,
    all_x, all_dy, all_meta, oh, recv_x, weighted, hid, gg, gu, so, dots, token_part,
    wg, wu, wd, rw, g, u, b, s, pg, pu, pb, ps, hg, hu, hb, hs, cg, cu, cb, cs,
    w_sem, z_send, z_recv, a_send, a_recv, b_send, b_recv, c_send, c_recv, d_send, d_recv,
):
    ep, me = lax.axis_index("ep"), lax.axis_index("tp")
    half = n_tp // 2
    parity = lax.rem(me, 2)
    mine = me // 2
    partner = {"tp": me + 1 - 2 * parity}
    others = [lax.rem(mine + d, half) for d in range(1, half)]
    places = [{"tp": 2 * j + parity} for j in others]
    eps = [lax.rem(ep + d, n_ep) for d in range(1, n_ep)]
    tok = x.shape[0]
    rows = g.shape[0] // n_tp
    s_rows = s.shape[0] // n_tp
    used = experts * per_expert
    loads = []
    for k, (src, dst) in enumerate(((w_gate, wg), (w_up, wu), (w_down, wd))):
        loads.append(pltpu.make_async_copy(src, dst, w_sem.at[k]))
        loads[-1].start()
    greet([{"ep": p} for p in eps] + [partner] + places)

    blocks = ((meta, all_meta), (x, all_x), (dy, all_dy))
    gathered = [[], [], []]
    for k, (src, dst) in enumerate(blocks):
        for d, p in enumerate(eps):
            c = remote(src, dst.at[ep], z_send.at[d, k], z_recv.at[d, k], {"ep": p})
            c.start()
            gathered[k].append(c)
    for src, dst in blocks:
        dst[ep] = src[...]
    if used < g.shape[0]:
        oh[...] = jnp.zeros_like(oh)
        rw[...] = jnp.zeros_like(rw)
        for ref in (g, u, b):
            ref[pl.ds(used, g.shape[0] - used), :] = jnp.zeros(
                (g.shape[0] - used, g.shape[1]), F32
            )
    for c in gathered[0]:
        c.wait_recv()
    e_rows = up_to(experts, 8)
    ids = (ep * experts + lax.broadcasted_iota(jnp.int32, (e_rows, tok), 0)).astype(F32)
    before = jnp.where(
        lax.broadcasted_iota(jnp.int32, (tok, tok), 0)
        < lax.broadcasted_iota(jnp.int32, (tok, tok), 1),
        1.0,
        0.0,
    ).astype(BF)
    place_in = lax.broadcasted_iota(jnp.int32, (per_expert, tok), 0).astype(F32)
    sums = [jnp.zeros((per_expert, 1), F32) for _ in range(experts)]
    for blk in range(n_ep):
        info = all_meta[blk]
        chosen = jnp.zeros((e_rows, tok), F32)
        weight_of = jnp.zeros((e_rows, tok), F32)
        for k in range(picks):
            same = info[k : k + 1, :] == ids
            chosen = jnp.where(same, 1.0, chosen)
            weight_of = jnp.where(same, info[picks + k : picks + k + 1, :], weight_of)
        rank = dot(chosen.astype(BF), before, 1, 0)
        slot = jnp.where(chosen > 0.0, rank + float(capacity * blk), -1.0)
        for e in range(experts):
            hot = place_in == slot[e : e + 1, :]
            oh[blk, pl.ds(e * per_expert, per_expert), :] = jnp.where(hot, 1.0, 0.0).astype(BF)
            sums[e] = sums[e] + jnp.sum(
                jnp.where(hot, weight_of[e : e + 1, :], 0.0), axis=1, keepdims=True
            )
    for e in range(experts):
        rw[pl.ds(e * per_expert, per_expert), :] = jnp.broadcast_to(sums[e], (per_expert, 128))

    full = (g, u, b, s)
    got = (pg, pu, pb, ps)
    held = (hg, hu, hb, hs)
    landed = (cg, cu, cb, cs)
    sizes = (rows, rows, rows, s_rows)

    def span(start, size):
        return pl.ds(pl.multiple_of(start * size, size), size)

    first = [None] * 4
    second = [[], [], [], []]

    def swap(k):
        first[k] = remote(
            full[k].at[span(1 - parity, half * sizes[k])],
            got[k],
            a_send.at[k],
            a_recv.at[k],
            partner,
        )
        first[k].start()

    def spread(k):
        first[k].wait()
        held[k][...] = (full[k][span(parity, half * sizes[k]), :] + got[k][...]).astype(BF)
        for d, j in enumerate(others):
            c = remote(
                held[k].at[span(j, sizes[k])],
                landed[k].at[d],
                b_send.at[d, k],
                b_recv.at[d, k],
                places[d],
            )
            c.start()
            second[k].append(c)

    def pick(source):
        total = dot(oh[0], source[0], 1, 0)
        for blk in range(1, n_ep):
            total = total + dot(oh[blk], source[blk], 1, 0)
        return total

    for c in gathered[1]:
        c.wait_recv()
    recv_x[...] = pick(all_x).astype(BF)
    for k, weight in ((0, wg), (1, wu)):
        loads[k].wait()
        for e in range(experts):
            at = pl.ds(e * per_expert, per_expert)
            full[k][at, :] = dot(recv_x[at, :], weight[e], 1, 0)
        swap(k)
    for blk in range(n_ep):
        s[pl.ds(blk * tok, tok), :] = dot(all_x[blk], s_in[...], 1, 1)
    spread(0)
    spread(1)
    for c in gathered[2]:
        c.wait_recv()
    recv_dy = pick(all_dy)
    weighted[...] = (rw[...][:, :1] * recv_dy).astype(BF)
    hid_dy = recv_dy.astype(BF)
    loads[2].wait()
    for e in range(experts):
        b[pl.ds(e * per_expert, per_expert), :] = dot(
            hid_dy[e * per_expert : (e + 1) * per_expert, :], wd[e], 1, 1
        )
    swap(2)
    for blk in range(n_ep):
        s[pl.ds(blk * tok, tok), :] += dot(all_dy[blk], s_in_back[...], 1, 1)
    swap(3)
    spread(2)
    spread(3)

    place = parity * half + mine

    def total(k):
        for c in second[k]:
            c.wait_recv()
        out = full[k][span(place, sizes[k]), :] + got[k][span(mine, sizes[k]), :]
        for d in range(half - 1):
            out = out + landed[k][d].astype(F32)
        return out

    last = []

    def share(k, ref, where):
        block = ref.at[where]
        for d in range(half - 1):
            c = remote(block, block, c_send.at[d, k], c_recv.at[d, k], places[d])
            c.start()
            last.append(c)
        c = remote(block, block, d_send.at[0, k], d_recv.at[0, k], partner)
        c.start()
        last.append(c)

    outs = ((hid, rows), (gg, rows), (gu, rows), (dots, 1), (so, s_rows))

    def part(k, index):
        return pl.ds(index, 1) if k == 3 else span(index, outs[k][1])

    gate, up, back = total(0), total(1), total(2)
    silu_out, silu_slope = silu_parts(gate)
    hidden = (silu_out * up).astype(BF)
    mine_rows = span(place, rows)
    dhidden = rw[mine_rows, :][:, :1] * back
    hid[mine_rows, :] = hidden
    gg[mine_rows, :] = (dhidden * up * silu_slope).astype(BF)
    gu[mine_rows, :] = (dhidden * silu_out).astype(BF)
    dots[place] = dot(
        jnp.ones((8, gate.shape[1]), F32),
        hidden.astype(F32) * back,
        1,
        1,
        lax.Precision.HIGHEST,
    )
    for k in range(4):
        share(k, outs[k][0], part(k, place))

    both = total(3)
    width = both.shape[1]
    lane = lax.broadcasted_iota(jnp.int32, both.shape, 1)
    s_up = pltpu.roll(both, width - cols, 1)
    s_back = pltpu.roll(both, width - 2 * cols, 1)
    s_out, s_slope = silu_parts(both)
    s_dgate = pltpu.roll(s_back * s_up * s_slope, cols, 1)
    s_dup = pltpu.roll(s_back * s_out, 2 * cols, 1)
    so[span(place, s_rows), :] = jnp.where(
        lane < cols, s_out * s_up, jnp.where(lane < 2 * cols, s_dgate, s_dup)
    ).astype(BF)
    share(4, so, part(4, place))

    def forward(k):
        ref = outs[k][0]
        for d in range(half - 1):
            source = lax.rem(mine + half - 1 - d, half)
            block = ref.at[part(k, parity * half + source)]
            remote(
                block, block, c_send.at[d, k], c_recv.at[d, k], places[d]
            ).wait_recv()
            c = remote(block, block, d_send.at[1 + d, k], d_recv.at[1 + d, k], partner)
            c.start()
            last.append(c)

    def settle(k):
        ref = outs[k][0]
        for d in range(half):
            source = mine if d == 0 else lax.rem(mine + half - d, half)
            block = ref.at[part(k, (1 - parity) * half + source)]
            remote(block, block, d_send.at[d, k], d_recv.at[d, k], partner).wait_recv()

    for k in range(4):
        forward(k)
    for k in range(4):
        settle(k)
    row_grad = []
    for e in range(experts):
        at = pl.ds(e * per_expert, per_expert)
        row_grad.append(
            (dot(gg[at, :], wg[e], 1, 1) + dot(gu[at, :], wu[e], 1, 1)).astype(BF)
        )
    if used < g.shape[0]:
        row_grad.append(jnp.zeros((g.shape[0] - used, x.shape[1]), BF))
    row_grad = jnp.concatenate(row_grad, axis=0)
    forward(4)
    settle(4)
    for blk in range(n_ep):
        token_part[blk] = (
            dot(oh[blk], row_grad, 0, 0)
            + dot(so[pl.ds(blk * tok, tok), :], s_out_w[...], 1, 0)
        ).astype(BF)
    for group in second:
        for c in group:
            c.wait_send()
    for group in gathered:
        for c in group:
            c.wait_send()
    for c in last:
        c.wait_send()


def row_squares(square):
    ones = jnp.ones((8, square.shape[1]), BF)
    high = square.astype(BF)
    low = (square - high.astype(F32)).astype(BF)
    return (dot(ones, high, 1, 1) + dot(ones, low, 1, 1))[:1, :]


def weights_kernel(
    experts, cols,
    recv_x, weighted, hid, gg, gu, all_x, all_dy, so,
    gate_out, up_out, down_out, sg_out, su_out, sd_out, gate_sq, up_sq, over_tp, over_ep,
):
    e = pl.program_id(0)
    gate = dot(recv_x[...], gg[...], 0, 0)
    gate_out[0] = gate
    gate_sq[pl.ds(e, 1), :] = row_squares(gate * gate)
    up = dot(recv_x[...], gu[...], 0, 0)
    up_out[0] = up
    up_sq[pl.ds(e, 1), :] = row_squares(up * up)
    down = dot(hid[...], weighted[...], 0, 0)
    down_out[0] = down

    @pl.when(e == 0)
    def _():
        over_tp[...] = jnp.zeros_like(over_tp)
        over_ep[...] = jnp.zeros_like(over_ep)
        pair = dot(so[...], all_x[...], 0, 0)
        sg, su = pair[cols : 2 * cols, :], pair[2 * cols : 3 * cols, :]
        sg_out[...] = sg
        su_out[...] = su
        over_ep[0:1, :] = jnp.sum(sg * sg, axis=0, keepdims=True)
        over_ep[1:2, :] = jnp.sum(su * su, axis=0, keepdims=True)
        sd_full = dot(so[...], all_dy[...], 0, 0)
        sd_out[...] = sd_full[:cols, :]
        sq = row_squares(sd_full * sd_full)
        kept = lax.broadcasted_iota(jnp.int32, sq.shape, 1) < cols
        sq = jnp.where(kept, sq, 0.0)
        span = min(over_tp.shape[1], sq.shape[1])
        over_tp[experts : experts + 1, :span] = sq[:, :span]

    over_tp[pl.ds(e, 1), :] = row_squares(down * down)


def finish_kernel(
    n_ep, n_tp, wg, es, ts, wg_out, es_out, ts_out,
    wg_in, es_in, ts_in, e_send, e_recv, t_send, t_recv,
):
    ep, tp = lax.axis_index("ep"), lax.axis_index("tp")
    eps = [lax.rem(ep + d, n_ep) for d in range(1, n_ep)]
    tps = [lax.rem(tp + d, n_tp) for d in range(1, n_tp)]
    greet([{"ep": p} for p in eps] + [{"tp": p} for p in tps])
    copies = []
    for d, p in enumerate(eps):
        for k, (src, dst) in enumerate(((wg.at[p], wg_in.at[d]), (es, es_in.at[d]))):
            copies.append(remote(src, dst, e_send.at[d, k], e_recv.at[d, k], {"ep": p}))
            copies[-1].start()
    for d, p in enumerate(tps):
        copies.append(remote(ts, ts_in.at[d], t_send.at[d], t_recv.at[d], {"tp": p}))
        copies[-1].start()
    for c in copies:
        c.wait()
    weights = wg[ep]
    norms = es[...]
    for d in range(n_ep - 1):
        weights = weights + wg_in[d]
        norms = norms + es_in[d]
    wg_out[...] = weights
    es_out[...] = norms
    down = ts[...]
    for d in range(n_tp - 1):
        down = down + ts_in[d]
    ts_out[...] = down


def call(kernel, collective, outs, scratch, *args, specs=None):
    return pl.pallas_call(
        kernel,
        out_shape=[jax.ShapeDtypeStruct(s, t) for s, t in outs],
        in_specs=specs or [VMEM] * len(args),
        out_specs=[VMEM] * len(outs),
        scratch_shapes=scratch,
        compiler_params=pltpu.CompilerParams(
            collective_id=collective,
            has_side_effects=True,
            vmem_limit_bytes=48 * 1024 * 1024,
        ),
    )(*args)


def per_device(
    n_ep, n_tp,
    tokens, cotangent, routes, gate_weights,
    expert_gate, expert_up, expert_down,
    shared_gate, shared_up, shared_down,
):
    dma = pltpu.SemaphoreType.DMA
    half = n_tp // 2
    tok_rows, narrow = tokens.shape
    picks = routes.shape[1]
    experts, _, ff = expert_gate.shape
    experts_all = experts * n_ep
    capacity = max(2, (tok_rows * picks + experts_all - 1) // experts_all)
    every = tok_rows * n_ep
    cols = shared_gate.shape[1] // n_ep
    ep = lax.axis_index("ep")
    per_expert = up_to(capacity * n_ep, 16)
    used = experts * per_expert
    rows = up_to(used, 16 * n_tp)
    width = up_to(3 * cols, 128)
    chunk, s_chunk = rows // n_tp, every // n_tp

    meta = jnp.concatenate([routes.astype(F32).T, gate_weights.T], axis=0)
    meta = jnp.pad(meta, ((0, up_to(2 * picks, 8) - 2 * picks), (0, 0)))
    sg = lax.dynamic_slice_in_dim(shared_gate.T, ep * cols, cols, 0)
    su = lax.dynamic_slice_in_dim(shared_up.T, ep * cols, cols, 0)
    sd = lax.dynamic_slice_in_dim(shared_down, ep * cols, cols, 0)
    s_in = jnp.pad(jnp.concatenate([sg, su], axis=0), ((0, width - 2 * cols), (0, 0)))
    s_in_back = jnp.pad(sd, ((2 * cols, width - 3 * cols), (0, 0)))
    s_out_w = jnp.pad(jnp.concatenate([sg, su], axis=0), ((cols, width - 3 * cols), (0, 0)))
    anywhere = pl.BlockSpec(memory_space=pl.ANY)
    vm = pltpu.VMEM
    (
        all_x, all_dy, all_meta, onehot, recv_x, weighted,
        hidden, grad_gate, grad_up, s_all, dots, token_part,
    ) = call(
        functools.partial(
            front_kernel, n_ep, n_tp, experts, per_expert, capacity, picks, cols
        ),
        0,
        [
            ((n_ep, tok_rows, narrow), BF),
            ((n_ep, tok_rows, narrow), BF),
            ((n_ep,) + meta.shape, F32),
            ((n_ep, rows, tok_rows), BF),
            ((rows, narrow), BF),
            ((rows, narrow), BF),
            ((rows, ff), BF),
            ((rows, ff), BF),
            ((rows, ff), BF),
            ((every, width), BF),
            ((n_tp, 8, chunk), F32),
            ((n_ep, tok_rows, narrow), BF),
        ],
        [
            vm(expert_gate.shape, BF), vm(expert_up.shape, BF), vm(expert_down.shape, BF),
            vm((rows, 128), F32),
        ]
        + [vm((rows, ff), F32)] * 3 + [vm((every, width), F32)]
        + [vm((rows // 2, ff), F32)] * 3 + [vm((every // 2, width), F32)]
        + [vm((rows // 2, ff), BF)] * 3 + [vm((every // 2, width), BF)]
        + [vm((half - 1, chunk, ff), BF)] * 3 + [vm((half - 1, s_chunk, width), BF)]
        + [
            dma((3,)), dma((n_ep - 1, 3)), dma((n_ep - 1, 3)),
            dma((4,)), dma((4,)), dma((half - 1, 4)), dma((half - 1, 4)),
            dma((half - 1, 5)), dma((half - 1, 5)), dma((half, 5)), dma((half, 5)),
        ],
        tokens, cotangent, meta, expert_gate, expert_up, expert_down,
        s_in, s_in_back, s_out_w,
        specs=[VMEM] * 3 + [anywhere] * 3 + [VMEM] * 3,
    )
    token_grad = token_part[ep].astype(F32)
    for d in range(1, n_ep):
        moved = lax.ppermute(
            lax.dynamic_index_in_dim(token_part, lax.rem(ep + d, n_ep), 0, False),
            "ep",
            [(i, (i + d) % n_ep) for i in range(n_ep)],
        )
        token_grad = token_grad + moved.astype(F32)
    token_grad = token_grad.astype(BF)

    whole_x = all_x.reshape(every, narrow)
    whole_dy = all_dy.reshape(every, narrow)
    norm_rows = up_to(experts + 1, 8)

    def fixed(shape):
        return pl.BlockSpec(shape, lambda e: (0,) * len(shape))

    def rowed(columns):
        return pl.BlockSpec((per_expert, columns), lambda e: (e, 0))

    def stacked(a, c):
        return pl.BlockSpec((1, a, c), lambda e: (e, 0, 0))

    flops = 2 * experts * per_expert * narrow * ff * 3 + 4 * every * narrow * width
    (
        gate_wgrad, up_wgrad, down_grad, sg_grad, su_grad, sd_grad,
        gate_rows_sq, up_rows_sq, over_tp, over_ep,
    ) = pl.pallas_call(
        functools.partial(weights_kernel, experts, cols),
        grid=(experts,),
        in_specs=[rowed(narrow), rowed(narrow), rowed(ff), rowed(ff), rowed(ff)]
        + [fixed(whole_x.shape), fixed(whole_dy.shape), fixed(s_all.shape)],
        out_specs=[stacked(narrow, ff), stacked(narrow, ff), stacked(ff, narrow)]
        + [fixed((cols, narrow))] * 3
        + [fixed((experts, narrow))] * 2
        + [fixed((norm_rows, ff)), fixed((8, narrow))],
        out_shape=[
            jax.ShapeDtypeStruct(shape, F32)
            for shape in (
                (experts, narrow, ff), (experts, narrow, ff), (experts, ff, narrow),
                (cols, narrow), (cols, narrow), (cols, narrow),
                (experts, narrow), (experts, narrow), (norm_rows, ff), (8, narrow),
            )
        ],
        cost_estimate=pl.CostEstimate(
            flops=flops, bytes_accessed=experts * narrow * ff * 12, transcendentals=0
        ),
        compiler_params=pltpu.CompilerParams(
            dimension_semantics=("arbitrary",), vmem_limit_bytes=48 * 1024 * 1024
        ),
    )(recv_x, weighted, hidden, grad_gate, grad_up, whole_x, whole_dy, s_all)

    ids = (ep * experts + jnp.arange(experts, dtype=jnp.int32)).astype(F32)
    match = all_meta[:, :picks, None, :] == ids[None, None, :, None]
    hot = onehot[:, :used].reshape(n_ep, experts, per_expert, tok_rows)
    row_dots = dots[:, 0, :].reshape(rows)[:used].reshape(1, experts, per_expert, 1)
    dot_of = jnp.sum(hot.astype(F32) * row_dots, axis=2)
    weight_part = jnp.sum(jnp.where(match, dot_of[:, None], 0.0), axis=2)
    weight_part = jnp.pad(weight_part, ((0, 0), (0, up_to(picks, 8) - picks), (0, 0)))
    peers, t_peers = n_ep - 1, n_tp - 1
    weight_grad, over_ep, over_tp = call(
        functools.partial(finish_kernel, n_ep, n_tp),
        1,
        [(weight_part.shape[1:], F32), (over_ep.shape, F32), (over_tp.shape, F32)],
        [
            vm((peers,) + weight_part.shape[1:], F32),
            vm((peers,) + over_ep.shape, F32),
            vm((t_peers,) + over_tp.shape, F32),
            dma((peers, 2)), dma((peers, 2)), dma((t_peers,)), dma((t_peers,)),
        ],
        weight_part, over_ep, over_tp,
    )
    return (
        token_grad,
        weight_grad[:picks].T,
        gate_wgrad,
        up_wgrad,
        down_grad,
        sg_grad.T,
        su_grad.T,
        sd_grad,
        gate_rows_sq,
        up_rows_sq,
        over_tp[:experts],
        over_ep[0],
        over_ep[1],
        over_tp[experts, :cols],
    )


def solution(mesh):
    n_ep, n_tp = mesh.shape["ep"], mesh.shape["tp"]
    return jax.shard_map(
        functools.partial(per_device, n_ep, n_tp),
        mesh=mesh,
        in_specs=(
            P("ep", "tp"),
            P("ep", "tp"),
            P("ep", None),
            P("ep", None),
            P("ep", "tp", None),
            P("ep", "tp", None),
            P("ep", None, "tp"),
            P("tp", None),
            P("tp", None),
            P(None, "tp"),
        ),
        out_specs=(
            P("ep", "tp"),
            P("ep", None),
            P("ep", "tp", None),
            P("ep", "tp", None),
            P("ep", None, "tp"),
            P("tp", "ep"),
            P("tp", "ep"),
            P("ep", "tp"),
            P("ep", "tp"),
            P("ep", "tp"),
            P("ep", None),
            P("tp"),
            P("tp"),
            P("ep"),
        ),
        check_vma=False,
    )
```

time: 99.7 us -> 79.7 us (0.80)
  matrix products: 23.4 us -> 0 us
  starting transfers between devices: 0 us -> 4.17 us
    dot_general x16 -> x0, matrix products: 23.4 us -> none  [the longest x1 3.1 us: per_device(): jnp.einsum('erf,erl->efl', hidden, weighted, preferred_element_type=F32)]
    pallas_call x3 -> x2, Pallas kernels: 59.4 us -> 51.2 us  [call(): pl.pallas_call(kernel, out_shape=[jax.ShapeDtypeStruct(s, t) for s, t in...]
    pallas_call x0 -> x1, Pallas kernels: none -> 7.7 us  [per_device(): pl.pallas_call(functools.partial(weights_kernel, experts, cols), grid=(ex...]
    ppermute x0 -> x3, starting transfers between devices: none -> 4.17 us  [per_device(): lax.ppermute(lax.dynamic_index_in_dim(token_part, lax.rem(ep + d, n_ep),...]
    reduce_sum x4 -> x1, other arithmetic: 1.98 us -> 0.31 us  [per_device(): dot_of = jnp.sum(hot.astype(F32) * row_dots, axis=2)]
    convert_element_type x1, other arithmetic: 0.69 us -> 1.69 us  [per_device(): token_grad = token_grad.astype(BF)]
    unnamed x25 -> x27, local copies, waits for them, and re-layouts: 7.29 us -> 6.41 us
  transfers between devices with their start and end apart: 0 -> 3, of which waited for: 0 -> 0; matrix products, arithmetic and copies ran while one was open for 0% -> 5% of each run, Pallas kernels for 0% -> 18%
where the time goes in v2:
time: 79.7 us; the launch traced here: 79.3 us
  Pallas kernels  58.9 us (74%)
  local copies, waits for them, and re-layouts  10.7 us (13%)
  other arithmetic  4.69 us (6%)
  starting transfers between devices  4.17 us (5%)
  between operations  0.84 us (1%)
    pallas_call x2, Pallas kernels, call(): pl.pallas_call(kernel, out_shape=[jax.ShapeDtypeStruct(s, t) for s, t in...  51.2 us
    pallas_call x1, Pallas kernels, per_device(): pl.pallas_call(functools.partial(weights_kernel, experts, cols), grid=(ex...  7.7 us
    unnamed x27, local copies, waits for them, and re-layouts  6.41 us
    ppermute x3, starting transfers between devices, per_device(): lax.ppermute(lax.dynamic_index_in_dim(token_part, lax.rem(ep + d, n_ep),...  4.17 us
    convert_element_type x1, other arithmetic, per_device(): token_grad = token_grad.astype(BF)  1.69 us
  transfers between devices with their start and end apart: 3, of which 0 were waited for; matrix products, arithmetic and copies ran while one was open for 5% of the time, Pallas kernels for 18%

profile of v2, /device:TPU:0, one launch (start us, length us, event | category | flops | bytes accessed | tf_op | source)
XLA Modules:
  0.0 79.3 jit_solution(791651854833213691)
XLA Ops:
  0.6 0.0 copy-start
  0.7 0.7 convert_bitcast_fusion
  1.4 0.2 copy-done
  1.6 0.9 %dynamic-slice_bitcast_fusion.3 = (bf16[144,256]{1,0:T(8,128)(2,1)S(1)}, bf16[144,256]{1,0:T(8,128)(2,1)S(1)}) fusion(bf16[256,576]{0,1:T(8,128)(2,1)} %param.18, s32[]{:T(128)S(6)} %select_n.22, bf16[256,576]{0,1:T(8,128)(2,1)} %param.17), kind=kLoop, calls=%fused_computation.10 | loop fusion | bytes 294916 | tf_op jit(solution)/shard_map/dynamic_slice | solution.py:418
  2.6 0.7 select_maximum_fusion.meta
  3.4 0.0 copy-start.11
  3.4 0.9 %copy-done.11 = bf16[160,256]{1,0:T(8,128)(2,1)S(1)} copy-done((bf16[160,256]{1,0:T(8,128)(2,1)S(1)}, bf16[160,256]{1,0:T(8,128)(2,1)}, u32[]{:S(2)}) %copy-start.11) | copy-done | bytes 81944
  4.3 44.8 %shard_map.209 = (bf16[4,160,256]{2,1,0:T(8,128)(2,1)S(1)}, bf16[4,160,256]{2,1,0:T(8,128)(2,1)S(1)}, f32[4,8,160]{2,1,0:T(8,128)S(1)}, bf16[4,384,160]{2,1,0:T(...) custom-call(bf16[160,256]{1,0:T(8,128)(2,1)S(1)} %copy-done.10, ...), custom_call_target="tpu_custom_call" | custom-call | tf_op jit(solution)/shard_map/pallas_call | solution.py:379
  49.1 0.0 copy-start.4
  49.1 0.7 copy-done.4
  49.8 0.7 copy-done.6
  50.5 0.7 copy-done.8
  51.2 0.7 copy-done.1
  51.9 0.7 dynamic-slice_bitcast_fusion.2
  52.6 2.5 %collective-permute-start = (bf16[160,256]{1,0:T(8,128)(2,1)}, bf16[160,256]{1,0:T(8,128)(2,1)}, u32[]{:S(2)}, u32[]{:S(2)}) collective-permute-start(bf16[160,256]{1,0:T(8,128)(2,1)} %get-tuple-element.64), channel_id=1, source_target_pairs={{0,8},{8,16},{16,24},{24,0},{1,9},{9,17},{17,25},{25,1},{2,10},{10... | collective-permute-start | bytes 245768 | tf_op jit(solution)/shard_map/ppermute | solution.py:466
  55.1 1.3 %collective-permute-start.2 = (bf16[160,256]{1,0:T(8,128)(2,1)}, bf16[160,256]{1,0:T(8,128)(2,1)}, u32[]{:S(2)}, u32[]{:S(2)}) collective-permute-start(bf16[160,256]{1,0:T(8,128)(2,1)} %get-tuple-element.65), channel_id=1, source_target_pairs={{0,24},{8,0},{16,8},{24,16},{1,25},{9,1},{17,9},{25,17},{2,26},{10... | collective-permute-start | bytes 245768 | tf_op jit(solution)/shard_map/ppermute | solution.py:466
  56.4 0.3 collective-permute-start.1
  56.7 0.5 add_convert_fusion
  57.3 0.8 slice_reduce_fusion
  58.0 0.1 mul.20
  58.1 0.3 fusion
  58.5 0.7 select_reduce_fusion
  59.2 0.0 copy-start.3
  59.3 1.0 %copy-done.3 = bf16[4,160,256]{2,1,0:T(8,128)(2,1)S(1)} copy-done((bf16[4,160,256]{2,1,0:T(8,128)(2,1)S(1)}, bf16[4,160,256]{2,1,0:T(8,128)(2,1)}, u32[]{:S(2)}) %copy-start.3) | copy-done | bytes 327704
  60.2 0.9 %copy-done.9 = bf16[384,256]{1,0:T(8,128)(2,1)S(1)} copy-done((bf16[384,256]{1,0:T(8,128)(2,1)S(1)}, bf16[384,256]{1,0:T(8,128)(2,1)}, u32[]{:S(2)}) %copy-start.9) | copy-done | bytes 196632
  61.2 7.7 %shard_map.210 = (f32[6,256,512]{2,1,0:T(8,128)}, f32[6,256,512]{2,1,0:T(8,128)}, f32[6,512,256]{2,1,0:T(8,128)}, f32[144,256]{1,0:T(8,128)}, f32[144,256]{1,0:T...) custom-call(bf16[384,256]{1,0:T(8,128)(2,1)S(1)} %copy-done.7, ...), custom_call_target="tpu_custom_call" | custom-call | flops 637534208 | bytes 9437184 | tf_op jit(solution)/shard_map/pallas_call | solution.py:491
  68.9 6.4 %shard_map.211 = (f32[8,160]{1,0:T(8,128)S(1)}, f32[8,256]{1,0:T(8,128)S(1)}, f32[8,512]{1,0:T(8,128)S(1)}) custom-call(f32[4,8,160]{2,1,0:T(8,128)S(1)} %pad.24.wg, f32[8,256]{1,0:T(8,128)S(1)} %get-tuple-element.51.es, f32[8,512]{1,0:T(8,128)S(1)} %get-tuple-element.52.ts), custom_call_target="tpu_custom_call" | custom-call | tf_op jit(solution)/shard_map/pallas_call | solution.py:379
  75.3 0.6 slice_bitcast_fusion
  75.9 0.6 fusion.5
  76.4 0.6 slice.27
  77.0 1.7 %fusion.3 = bf16[160,256]{1,0:T(8,128)(2,1)} fusion(bf16[160,256]{1,0:T(8,128)(2,1)} %collective-permute-done.2, bf16[160,256]{1,0:T(8,128)(2,1)} %collective-permute-done.1, bf16[160,256]{1,0:T(8,128)(2,1)} %collective-permute-done, bf16[4,160,256]{2,1,0:T(8,128)(2,1)} %copy-done.1, s32[]{:T(128)S(6)} %select_n.23), kind=kLoop, calls=%fused_computation.5 | loop fusion | flops 327680 | bytes 409604 | tf_op jit(solution)/shard_map/convert_element_type | solution.py:472
  78.7 0.6 copy.30
  (26 shorter events, 0.1 us)
Async XLA Ops:
  0.6 1.0 %copy-start = (bf16[576,256]{1,0:T(8,128)(2,1)S(1)}, bf16[576,256]{1,0:T(8,128)(2,1)}, u32[]{:S(2)}) copy-start(bf16[576,256]{1,0:T(8,128)(2,1)} %param.19) | copy-start | bytes 884740
  0.7 2.7 %copy-start.10 = (bf16[160,256]{1,0:T(8,128)(2,1)S(1)}, bf16[160,256]{1,0:T(8,128)(2,1)}, u32[]{:S(2)}) copy-start(bf16[160,256]{1,0:T(8,128)(2,1)} %x.11) | copy-start | bytes 245764
  3.4 0.9 %copy-start.11 = (bf16[160,256]{1,0:T(8,128)(2,1)S(1)}, bf16[160,256]{1,0:T(8,128)(2,1)}, u32[]{:S(2)}) copy-start(bf16[160,256]{1,0:T(8,128)(2,1)} %dy.1) | copy-start | bytes 245764
  49.1 0.7 copy-start.4
  49.8 0.7 copy-start.6
  50.5 0.7 copy-start.8
  51.2 0.7 copy-start.1
  51.2 1.4 %copy-start.2 = (bf16[4,160,256]{2,1,0:T(8,128)(2,1)}, bf16[4,160,256]{2,1,0:T(8,128)(2,1)S(1)}, u32[]{:S(2)}) copy-start(bf16[4,160,256]{2,1,0:T(8,128)(2,1)S(1)} %get-tuple-element.48) | copy-start | bytes 983044
  51.2 1.4 %copy-start.12 = (f32[8,8,48]{2,1,0:T(8,128)}, f32[8,8,48]{2,1,0:T(8,128)S(1)}, u32[]{:S(2)}) copy-start(f32[8,8,48]{2,1,0:T(8,128)S(1)} %get-tuple-element.42) | copy-start | bytes 36868
  51.9 7.3 %copy-start.5 = (bf16[4,160,256]{2,1,0:T(8,128)(2,1)S(1)}, bf16[4,160,256]{2,1,0:T(8,128)(2,1)}, u32[]{:S(2)}) copy-start(bf16[4,160,256]{2,1,0:T(8,128)(2,1)} %copy-done.4) | copy-start | bytes 983044
  51.9 7.4 %copy-start.7 = (bf16[384,256]{1,0:T(8,128)(2,1)S(1)}, bf16[384,256]{1,0:T(8,128)(2,1)}, u32[]{:S(2)}) copy-start(bf16[384,256]{1,0:T(8,128)(2,1)} %copy-done.6) | copy-start | bytes 589828
  52.6 24.4 %collective-permute-start = (bf16[160,256]{1,0:T(8,128)(2,1)}, bf16[160,256]{1,0:T(8,128)(2,1)}, u32[]{:S(2)}, u32[]{:S(2)}) collective-permute-start(bf16[160,256]{1,0:T(8,128)(2,1)} %get-tuple-element.64), channel_id=1, source_target_pairs={{0,8},{8,16},{16,24},{24,0},{1,9},{9,17},{17,25},{25,1},{2,10},{10... | collective-permute-start | bytes 245768 | tf_op jit(solution)/shard_map/ppermute | solution.py:466
  55.1 21.9 %collective-permute-start.2 = (bf16[160,256]{1,0:T(8,128)(2,1)}, bf16[160,256]{1,0:T(8,128)(2,1)}, u32[]{:S(2)}, u32[]{:S(2)}) collective-permute-start(bf16[160,256]{1,0:T(8,128)(2,1)} %get-tuple-element.65), channel_id=1, source_target_pairs={{0,24},{8,0},{16,8},{24,16},{1,25},{9,1},{17,9},{25,17},{2,26},{10... | collective-permute-start | bytes 245768 | tf_op jit(solution)/shard_map/ppermute | solution.py:466
  56.4 20.6 %collective-permute-start.1 = (bf16[160,256]{1,0:T(8,128)(2,1)S(1)}, bf16[160,256]{1,0:T(8,128)(2,1)}, u32[]{:S(2)}, u32[]{:S(2)}) collective-permute-start(bf16[160,256]{1,0:T(8,128)(2,1)S(1)} %get-tuple-element.66), channel_id=1, source_target_pairs={{0,16},{8,24},{16,0},{24,8},{1,17},{9,25},{17,1},{25,9},{2,18},{10... | collective-permute-start | bytes 245768 | tf_op jit(solution)/shard_map/ppermute | solution.py:466
  59.2 1.0 %copy-start.3 = (bf16[4,160,256]{2,1,0:T(8,128)(2,1)S(1)}, bf16[4,160,256]{2,1,0:T(8,128)(2,1)}, u32[]{:S(2)}) copy-start(bf16[4,160,256]{2,1,0:T(8,128)(2,1)} %copy-done.2) | copy-start | bytes 983044
  60.2 0.9 %copy-start.9 = (bf16[384,256]{1,0:T(8,128)(2,1)S(1)}, bf16[384,256]{1,0:T(8,128)(2,1)}, u32[]{:S(2)}) copy-start(bf16[384,256]{1,0:T(8,128)(2,1)} %copy-done.8) | copy-start | bytes 589828
